TPU v7x, 512 devices: a whole 4x8x8 slice. The times are simulated.
512 devices in a mesh: sp: 256 (over z, y, x), tp: 2 (over core).
Axes of the slice: x: 4, y: 8, z: 8, core: 2. Of those that a mesh axis runs over, the one named last changes fastest.
Arguments:
- proj_a: bfloat16 [65536, 3072], P('sp', 'tp'), may hold values from -20 to 20
- proj_gate: bfloat16 [65536, 3072], P('sp', 'tp'), may hold values from -6 to 6
- taps: bfloat16 [31, 3072], P(None, 'tp'), may hold values from -1 to 1
- norm_gain: float32 [3072], P('tp'), may hold values from 0.1 to 1.9
- norm_shift: float32 [3072], P('tp'), may hold values from -3 to 3
- cotangent: bfloat16 [65536, 3072], P('sp', 'tp'), may hold values from -6 to 6
Outputs:
- a_grad: bfloat16 [65536, 3072], P('sp', 'tp')
- gate_grad: bfloat16 [65536, 3072], P('sp', 'tp')
- taps_grad: float32 [31, 3072], P(None, 'tp')
- gain_grad: float32 [3072], P('tp')
- shift_grad: float32 [3072], P('tp')
All inputs are finite; a program needn't handle non-finite values.
Results may differ from a plain program's by a relative error of at most 0.0048.
Values may be sent and summed in bfloat16 or wider, within the bound.
A program may use at most 64 MiB of HBM per device.

v0:
```python
import jax
import jax.numpy as jnp
from jax import lax
from jax.sharding import Mesh
from jax.sharding import PartitionSpec as P

D = 3072
SP = ("sp_0", "sp_1", "sp_2")


EPS = 1e-05


def total_of_pieces(x, axis):
    blocks = lax.all_gather(x, axis)
    return blocks.sum(axis=0)


def from_behind(x, axis, by):
    size = lax.axis_size(axis)
    pairs = [(i, i + by) for i in range(size) if 0 <= i + by < size]
    return lax.ppermute(x, axis, pairs)


def padded_to(lines, size):
    spare = -lines.shape[0] % size
    if not spare:
        return lines
    return jnp.concatenate([lines, jnp.zeros((spare, *lines.shape[1:]), lines.dtype)])


def from_everyone(x, axis):
    copies = jnp.broadcast_to(x, (lax.axis_size(axis), *x.shape))
    return lax.all_to_all(copies, axis, split_axis=0, concat_axis=0, tiled=True)


def joined_along(blocks, dim):
    dims = list(blocks.shape[1:])
    dims[dim] *= blocks.shape[0]
    return jnp.moveaxis(blocks, 0, dim).reshape(dims)


def gathered_by_axis(x, axes, dim):
    far, near = axes
    leading = from_everyone(x, far)
    blocks = jnp.swapaxes(from_everyone(leading, near), 0, 1)
    return joined_along(blocks.reshape(-1, *x.shape), dim)


def split_up(x, dim, size):
    dims = x.shape
    blocks = x.reshape(*dims[:dim], size, dims[dim] // size, *dims[dim + 1 :])
    return jnp.moveaxis(blocks, dim, 0)


def sent_and_summed(x, axis, dim):
    size = lax.axis_size(axis)
    blocks = lax.all_to_all(split_up(x, dim, size), axis, 0, 0, tiled=True)
    return jnp.sum(blocks, axis=0)


def sum_by_axis(x, axes, dim):
    far, near = axes
    own = sent_and_summed(split_up(x, dim, lax.axis_size(far)), near, dim + 1)
    return jnp.sum(lax.all_to_all(own, far, 0, 0, tiled=True), axis=0)


def nested_sum(x, axes):
    padded = padded_to(x, lax.axis_size(axes[0]) * lax.axis_size(axes[1]))
    whole = gathered_by_axis(sum_by_axis(padded, axes, 0), axes, 0)
    return lax.slice_in_dim(whole, 0, len(x)).reshape(x.shape)


def in_one(arrays, axis):
    vector, at, gathered = (jnp.concatenate([a.reshape(-1) for a in arrays]), 0, [])
    running = nested_sum(vector, axis)
    for a in arrays:
        gathered.append(running[at : at + a.size].reshape(a.shape))
        at += a.size
    return tuple(gathered)


def gated(a_rows, g_rows):
    return (a_rows.astype(jnp.float32) * jax.nn.sigmoid(g_rows.astype(jnp.float32))).astype(
        jnp.bfloat16
    )


def depthwise(source, tapf, count):
    total = jnp.zeros((count, source.shape[1]), jnp.float32)
    for k in range(tapf.shape[0]):
        total = total + tapf[k] * source[k : k + count].astype(jnp.float32)
    return total


def transposed(source, tapf, count):
    edge = tapf.shape[0] - 1
    total = jnp.zeros((count, source.shape[1]), jnp.float32)
    for k in range(tapf.shape[0]):
        total = total + tapf[edge - k] * source[k : k + count]
    return total


def norm_backward(conv, cot_rows, gain, shift):
    mean = total_of_pieces(jnp.sum(conv, axis=1, keepdims=True), "tp") / D
    cent = conv - mean
    spread = total_of_pieces(jnp.sum(cent * cent, axis=1, keepdims=True), "tp") / D
    rstd = lax.rsqrt(spread + EPS)
    normed = cent * rstd
    pre = normed * gain + shift
    sig = jax.nn.sigmoid(pre)
    dpre = cot_rows.astype(jnp.float32) * sig * (1.0 + pre * (1.0 - sig))
    dnormed = dpre * gain
    dn_sum, dn_dot = (
        total_of_pieces(jnp.sum(dnormed, axis=1, keepdims=True), "tp"),
        total_of_pieces(jnp.sum(dnormed * normed, axis=1, keepdims=True), "tp"),
    )
    dconv = rstd * (dnormed - dn_sum / D - normed * (dn_dot / D))
    return (dconv, dpre, normed)


def body(proj_a, proj_gate, taps, norm_gain, norm_shift, cotangent):
    width = taps.shape[0]
    edge = width - 1
    rows = proj_a.shape[0]
    chans = proj_a.shape[1]
    tapf = taps.astype(jnp.float32)
    glu = gated(proj_a, proj_gate)
    before = from_behind(glu[rows - edge :], SP, 1)
    glu_all = jnp.concatenate([before, glu], axis=0)
    conv = depthwise(glu_all, tapf, rows)
    dconv, dpre, normed = norm_backward(conv, cotangent, norm_gain, norm_shift)
    pad = jnp.zeros((edge, chans), jnp.float32)
    spread_rows = transposed(jnp.concatenate([pad, dconv, pad], axis=0), tapf, rows + edge)
    returned = from_behind(spread_rows[:edge], SP, -1)
    mine = spread_rows[edge:]
    dglu = jnp.concatenate([mine[: rows - edge], mine[rows - edge :] + returned], axis=0)
    taps_part = jnp.stack(
        [jnp.sum(dconv * glu_all[j : j + rows].astype(jnp.float32), axis=0) for j in range(width)]
    )
    gain_part = jnp.sum(dpre * normed, axis=0)
    shift_part = jnp.sum(dpre, axis=0)
    taps_grad, gain_grad, shift_grad = in_one(
        (taps_part, gain_part, shift_part), (("sp_0", "sp_1"), "sp_2")
    )
    sg = jax.nn.sigmoid(proj_gate.astype(jnp.float32))
    a_grad = (dglu * sg).astype(jnp.bfloat16)
    gate_grad = (dglu * proj_a.astype(jnp.float32) * sg * (1.0 - sg)).astype(jnp.bfloat16)
    return (a_grad, gate_grad, taps_grad, gain_grad, shift_grad)


def solution(mesh):
    torus = Mesh(mesh.devices.reshape(8, 8, 4, mesh.shape["tp"]), ("sp_0", "sp_1", "sp_2", "tp"))
    return jax.shard_map(
        body,
        mesh=torus,
        in_specs=(P(SP, "tp"), P(SP, "tp"), P(None, "tp"), P("tp"), P("tp"), P(SP, "tp")),
        out_specs=(P(SP, "tp"), P(SP, "tp"), P(None, "tp"), P("tp"), P("tp")),
        check_vma=False,
    )
```

profile of v0, /device:TPU:8, one launch (start us, length us, event | category | flops | bytes accessed | tf_op | source)
XLA Modules:
  0.0 117.8 jit_solution(3946270337812381077)
XLA Ops:
  0.6 0.0 copy-start.5
  0.6 1.9 %fusion.30 = bf16[256,1536]{1,0:T(8,128)(2,1)S(1)} fusion(bf16[256,1536]{1,0:T(8,128)(2,1)} %param.6, bf16[256,1536]{1,0:T(8,128)(2,1)} %param.7), kind=kLoop, calls=%fused_computation.153 | loop fusion | flops 2752512 | bytes 2359296 | tf_op jit(solution)/shard_map/convert_element_type | solution.py:84
  2.5 3.4 %collective-permute-start = (bf16[30,1536]{1,0:T(8,128)(2,1)S(1)}, bf16[30,1536]{1,0:T(8,128)(2,1)S(1)}, u32[]{:S(2)}, u32[]{:S(2)}) collective-permute-start(bf16[30,1536]{1,0:T(8,128)(2,1)S(1)} %slice.462), channel_id=1, source_target_pairs={{0,2},{2,4},{4,6},{6,8},{8,10},{10,12},{12,14},{14,16},{16,18},{18... | collective-permute-start | bytes 276488 | tf_op jit(solution)/shard_map/ppermute | solution.py:22
  5.9 0.0 copy-done.5
  6.0 0.3 slice_reduce_fusion.29
  6.3 0.2 slice_reduce_fusion.28
  6.5 4.7 %collective-permute-done = bf16[30,1536]{1,0:T(8,128)(2,1)S(1)} collective-permute-done((bf16[30,1536]{1,0:T(8,128)(2,1)S(1)}, bf16[30,1536]{1,0:T(8,128)(2,1)S(1)}, u32[]{:S(2)}, u32[]{:S(2)}) %collective-permute-start) | collective-permute-done | bytes 92192 | tf_op jit(solution)/shard_map/ppermute | solution.py:22
  11.2 0.0 copy-start.4
  11.2 0.0 copy-start.6
  11.2 0.0 copy-start.7
  11.2 8.0 %fusion.124 = (f32[256]{0:T(256)S(1)}, f32[256,1536]{1,0:T(8,128)S(1)}) fusion(bf16[256,1536]{1,0:T(8,128)(2,1)S(1)} %fusion.30, f32[1536]{0:T(1024)S(1)} %get-tuple-element.70, bf16[30,1536]{1,0:T(8,128)(2,1)S(1)} %collective-permute-done, f32[1536]{0:T(1024)S(1)} %get-tuple-element.41, f32[1536]{0:T(1024)S(1)} %get-tuple-element.42, ...), kind=kLoop, calls=%fused_computation.296 | loop fusion | flops 71958272 | bytes 2642944 | tf_op jit(solution)/shard_map/reduce_sum | solution.py:105
  19.1 0.0 copy-start
  19.1 1.8 %all-gather.4 = f32[2,1,256]{2,1,0:T(1,128)S(1)} all-gather(f32[1,1,256]{2,1,0:T(1,128)S(1)} %bitcast.12), channel_id=2, replica_groups=mesh['sp_0'=8,'sp_1'=8,'sp_2'=4,'tp'=2] {'tp'}, dimensions={0}, use_global_device_ids=true | all-gather | bytes 3072 | tf_op jit(solution)/shard_map/all_gather | solution.py:15
  21.0 0.3 multiply_reduce_fusion.2
  21.3 1.8 %all-gather.5 = f32[2,1,256]{2,1,0:T(1,128)S(1)} all-gather(f32[1,1,256]{2,1,0:T(1,128)S(1)} %bitcast.15), channel_id=3, replica_groups=mesh['sp_0'=8,'sp_1'=8,'sp_2'=4,'tp'=2] {'tp'}, dimensions={0}, use_global_device_ids=true | all-gather | bytes 3072 | tf_op jit(solution)/shard_map/all_gather | solution.py:15
  23.1 0.0 copy-done.4
  23.1 0.0 copy-done.6
  23.1 0.0 copy-done.7
  23.1 2.5 %multiply_reduce_fusion = (f32[1536]{0:T(1024)S(1)}, f32[256]{0:T(256)S(1)}, f32[256]{0:T(256)S(1)}, f32[1536]{0:T(1024)S(1)}, f32[256,1536]{1,0:T(8,128)}) fusion(f32[256,1536]{1,0:T(8,128)S(1)} %get-tuple-element.74, f32[256]{0:T(256)S(1)} %add_rsqrt_fusion, f32[256]{0:T(256)S(1)} %broadcast_multiply_fusion.2, f32[1536]{0:T(1024)S(1)} %copy-done.6, ...), kind=kLoop, calls=%fused_computation.219 | loop fusion | flops 7860736 | bytes 3960832 | tf_op jit(solution)/shard_map/reduce_sum | solution.py:141
  25.7 0.0 copy-done
  25.7 1.8 %all-gather.7 = f32[2,1,256]{2,1,0:T(1,128)S(1)} all-gather(f32[1,1,256]{2,1,0:T(1,128)S(1)} %bitcast.14), channel_id=5, replica_groups=mesh['sp_0'=8,'sp_1'=8,'sp_2'=4,'tp'=2] {'tp'}, dimensions={0}, use_global_device_ids=true | all-gather | bytes 3072 | tf_op jit(solution)/shard_map/all_gather | solution.py:15
  27.5 1.8 %all-gather.6 = f32[2,1,256]{2,1,0:T(1,128)S(1)} all-gather(f32[1,1,256]{2,1,0:T(1,128)S(1)} %bitcast.13), channel_id=4, replica_groups=mesh['sp_0'=8,'sp_1'=8,'sp_2'=4,'tp'=2] {'tp'}, dimensions={0}, use_global_device_ids=true | all-gather | bytes 3072 | tf_op jit(solution)/shard_map/all_gather | solution.py:15
  29.4 3.6 %fusion.93 = (f32[1536]{0:T(1024)S(1)}, f32[1536]{0:T(1024)S(1)}, f32[1536]{0:T(1024)S(1)}, f32[1536]{0:T(1024)S(1)}, f32[1536]{0:T(1024)S(1)}, /*index=5*/f32[1...) fusion(bf16[256,1536]{1,0:T(8,128)(2,1)S(1)} %fusion.30, bf16[30,1536]{1,0:T(8,128)(2,1)S(1)} %collective-permute-done, ...), kind=kLoop, calls=%fused_computation.216 | loop fusion | flops 18077184 | bytes 5650432 | tf_op jit(solution)/shard_map/reduce_sum | solution.py:139
  33.0 1.4 %fusion.64 = (f32[1536]{0:T(1024)S(1)}, f32[1536]{0:T(1024)S(1)}, f32[1536]{0:T(1024)S(1)}, f32[1536]{0:T(1024)S(1)}, f32[1536]{0:T(1024)S(1)}, /*index=5*/f32[1536]{0:T(1024)S(1)}) fusion(f32[256,1536]{1,0:T(8,128)S(1)} %get-tuple-element.71, bf16[30,1536]{1,0:T(8,128)(2,1)S(1)} %collective-permute-done, bf16[256,1536]{1,0:T(8,128)(2,1)S(1)} %fusion.30), kind=kLoop, calls=%fused_computation.187 | loop fusion | flops 14146560 | bytes 2488320 | tf_op jit(solution)/shard_map/reduce_sum | solution.py:139
  34.5 1.4 %fusion.70 = (f32[1536]{0:T(1024)S(1)}, f32[1536]{0:T(1024)S(1)}, f32[1536]{0:T(1024)S(1)}, f32[1536]{0:T(1024)S(1)}, f32[1536]{0:T(1024)S(1)}, /*index=5*/f32[1536]{0:T(1024)S(1)}) fusion(f32[256,1536]{1,0:T(8,128)S(1)} %get-tuple-element.71, bf16[30,1536]{1,0:T(8,128)(2,1)S(1)} %collective-permute-done, bf16[256,1536]{1,0:T(8,128)(2,1)S(1)} %fusion.30), kind=kLoop, calls=%fused_computation.193 | loop fusion | flops 14146560 | bytes 2488320 | tf_op jit(solution)/shard_map/reduce_sum | solution.py:139
  35.9 1.4 %fusion.76 = (f32[1536]{0:T(1024)S(1)}, f32[1536]{0:T(1024)S(1)}, f32[1536]{0:T(1024)S(1)}, f32[1536]{0:T(1024)S(1)}, f32[1536]{0:T(1024)S(1)}, /*index=5*/f32[1536]{0:T(1024)S(1)}) fusion(f32[256,1536]{1,0:T(8,128)S(1)} %get-tuple-element.71, bf16[30,1536]{1,0:T(8,128)(2,1)S(1)} %collective-permute-done, bf16[256,1536]{1,0:T(8,128)(2,1)S(1)} %fusion.30), kind=kLoop, calls=%fused_computation.199 | loop fusion | flops 14146560 | bytes 2488320 | tf_op jit(solution)/shard_map/reduce_sum | solution.py:139
  37.4 1.4 %fusion.82 = (f32[1536]{0:T(1024)S(1)}, f32[1536]{0:T(1024)S(1)}, f32[1536]{0:T(1024)S(1)}, f32[1536]{0:T(1024)S(1)}, f32[1536]{0:T(1024)S(1)}, /*index=5*/f32[1536]{0:T(1024)S(1)}) fusion(f32[256,1536]{1,0:T(8,128)S(1)} %get-tuple-element.71, bf16[30,1536]{1,0:T(8,128)(2,1)S(1)} %collective-permute-done, bf16[256,1536]{1,0:T(8,128)(2,1)S(1)} %fusion.30), kind=kLoop, calls=%fused_computation.205 | loop fusion | flops 14146560 | bytes 2488320 | tf_op jit(solution)/shard_map/reduce_sum | solution.py:139
  39.1 0.3 stack.127
  39.4 0.4 reshape_reshape.6
  39.8 0.8 copy.11
  40.6 3.4 %all-to-all-start = ((f32[4,64,198]{2,1,0:T(8,128)}), f32[4,64,198]{2,1,0:T(8,128)S(1)}, u32[]{:S(2)}, u32[]{:S(2)}) async-start(f32[4,64,198]{2,1,0:T(8,128)} %copy.11), calls=%async_computation | async-start | bytes 524288 | tf_op jit(solution)/shard_map/all_to_all | solution.py:58
  44.0 0.2 pad_maximum_fusion
  44.2 6.8 %fusion.1 = f32[286,1536]{1,0:T(8,128)S(1)} fusion(f32[316,1536]{1,0:T(8,128)S(1)} %pad_maximum_fusion, f32[256,1536]{1,0:T(8,128)S(1)} %get-tuple-element.71, f32[1536]{0:T(1024)S(1)} %get-tuple-element.40, f32[1536]{0:T(1024)S(1)} %get-tuple-element.59, f32[1536]{0:T(1024)S(1)} %get-tuple-element.69, f32[1536]{0:T(1024)S(1)} %get-tuple-element.68, ...), kind=kLoop, calls=%fused_computation.96 | loop fusion | flops 26797056 | bytes 54478848 | tf_op jit(solution)/shard_map/add | solution.py:100
  51.0 0.0 copy-start.1
  51.0 1.2 %copy-done.1 = f32[286,1536]{1,0:T(8,128)} copy-done((f32[286,1536]{1,0:T(8,128)}, f32[286,1536]{1,0:T(8,128)S(1)}, u32[]{:S(2)}) %copy-start.1) | copy-done | bytes 1757208
  52.3 5.5 %collective-permute-start.1 = (f32[30,1536]{1,0:T(8,128)S(1)}, f32[30,1536]{1,0:T(8,128)}, u32[]{:S(2)}, u32[]{:S(2)}) collective-permute-start(f32[30,1536]{1,0:T(8,128)S(1)} %slice.581), channel_id=1, source_target_pairs={{2,0},{4,2},{6,4},{8,6},{10,8},{12,10},{14,12},{16,14},{18,16},{20... | collective-permute-start | bytes 552968 | tf_op jit(solution)/shard_map/ppermute | solution.py:22
  57.8 0.0 all-to-all-done
  57.8 0.7 all_to_all.19
  58.5 17.4 %all-to-all-start.1 = ((f32[64,1,198]{2,1,0:T(1,128)}), f32[64,1,198]{2,1,0:T(1,128)S(1)}, u32[]{:S(2)}, u32[]{:S(2)}) async-start(f32[64,1,198]{2,1,0:T(1,128)} %all_to_all.19), calls=%async_computation.1 | async-start | bytes 131072 | tf_op jit(solution)/shard_map/all_to_all | solution.py:65
  75.9 1.5 %slice.579 = f32[226,1536]{1,0:T(8,128)S(1)} slice(f32[286,1536]{1,0:T(8,128)} %copy-done.1), slice={[30:256], [0:1536]} | slice | bytes 2777088 | tf_op jit(solution)/shard_map/slice | solution.py:137
  77.4 0.0 copy-start.2
  77.4 0.0 copy-start.3
  77.4 9.9 %all-to-all-done.1 = f32[64,1,198]{2,1,0:T(1,128)S(1)} async-done(((f32[64,1,198]{2,1,0:T(1,128)}), f32[64,1,198]{2,1,0:T(1,128)S(1)}, u32[]{:S(2)}, u32[]{:S(2)}) %all-to-all-start.1) | async-done | bytes 50720 | tf_op jit(solution)/shard_map/all_to_all | solution.py:65
  87.3 0.1 reduce_sum.429
  87.4 0.7 broadcast_in_dim.13
  88.0 5.3 %all-to-all-start.2 = ((f32[64,1,198]{2,1,0:T(1,128)}), f32[64,1,198]{2,1,0:T(1,128)S(1)}, u32[]{:S(2)}, u32[]{:S(2)}) async-start(f32[64,1,198]{2,1,0:T(1,128)} %broadcast_in_dim.13), calls=%async_computation.2 | async-start | bytes 131072 | tf_op jit(solution)/shard_map/all_to_all | solution.py:34
  93.4 0.0 collective-permute-done.1
  93.4 1.0 slice_add_fusion
  94.4 10.4 %all-to-all-done.2 = f32[64,1,198]{2,1,0:T(1,128)S(1)} async-done(((f32[64,1,198]{2,1,0:T(1,128)}), f32[64,1,198]{2,1,0:T(1,128)S(1)}, u32[]{:S(2)}, u32[]{:S(2)}) %all-to-all-start.2) | async-done | bytes 50720 | tf_op jit(solution)/shard_map/all_to_all | solution.py:34
  104.9 0.7 broadcast_in_dim.14
  105.6 3.4 %all-to-all-start.3 = ((f32[4,64,198]{2,1,0:T(8,128)}), f32[4,64,198]{2,1,0:T(8,128)S(1)}, u32[]{:S(2)}, u32[]{:S(2)}) async-start(f32[4,64,198]{2,1,0:T(8,128)} %broadcast_in_dim.14), calls=%async_computation.3 | async-start | bytes 524288 | tf_op jit(solution)/shard_map/all_to_all | solution.py:34
  109.0 0.0 copy-done.2
  109.0 0.0 copy-done.3
  109.0 1.8 %fusion.33 = (bf16[256,1536]{1,0:T(8,128)(2,1)}, bf16[256,1536]{1,0:T(8,128)(2,1)}) fusion(bf16[256,1536]{1,0:T(8,128)(2,1)S(1)} %copy-done.2, f32[30,1536]{1,0:T(8,128)S(1)} %slice_add_fusion, f32[226,1536]{1,0:T(8,128)S(1)} %slice.579, bf16[256,1536]{1,0:T(8,128)(2,1)S(1)} %copy-done.3), kind=kLoop, calls=%fused_computation.156 | loop fusion | flops 5111808 | bytes 4718592 | tf_op jit(solution)/shard_map/convert_element_type | solution.py:148
  110.8 4.8 %all-to-all-done.3 = f32[4,64,198]{2,1,0:T(8,128)S(1)} async-done(((f32[4,64,198]{2,1,0:T(8,128)}), f32[4,64,198]{2,1,0:T(8,128)S(1)}, u32[]{:S(2)}, u32[]{:S(2)}) %all-to-all-start.3) | async-done | bytes 202784 | tf_op jit(solution)/shard_map/all_to_all | solution.py:34
  115.6 0.2 copy.12
  115.8 0.4 slice.456
  116.2 0.3 reshape_reshape.7
  116.5 0.7 slice.582
  117.2 0.6 fusion.126
  (47 shorter events, 0.4 us)
Async XLA Ops:
  0.6 5.3 %copy-start.5 = (bf16[31,1536]{1,0:T(8,128)(2,1)S(1)}, bf16[31,1536]{1,0:T(8,128)(2,1)}, u32[]{:S(2)}) copy-start(bf16[31,1536]{1,0:T(8,128)(2,1)} %param.8) | copy-start | bytes 285700
  2.5 8.6 %collective-permute-start = (bf16[30,1536]{1,0:T(8,128)(2,1)S(1)}, bf16[30,1536]{1,0:T(8,128)(2,1)S(1)}, u32[]{:S(2)}, u32[]{:S(2)}) collective-permute-start(bf16[30,1536]{1,0:T(8,128)(2,1)S(1)} %slice.462), channel_id=1, source_target_pairs={{0,2},{2,4},{4,6},{6,8},{8,10},{10,12},{12,14},{14,16},{16,18},{18... | collective-permute-start | bytes 276488 | tf_op jit(solution)/shard_map/ppermute | solution.py:22
  11.2 12.0 %copy-start.4 = (bf16[256,1536]{1,0:T(8,128)(2,1)S(1)}, bf16[256,1536]{1,0:T(8,128)(2,1)}, u32[]{:S(2)}) copy-start(bf16[256,1536]{1,0:T(8,128)(2,1)} %param.11) | copy-start | bytes 2359300
  11.2 12.0 %copy-start.6 = (f32[1536]{0:T(1024)S(1)}, f32[1536]{0:T(1024)}, u32[]{:S(2)}) copy-start(f32[1536]{0:T(1024)} %param.9) | copy-start | bytes 18436
  11.2 12.0 %copy-start.7 = (f32[1536]{0:T(1024)S(1)}, f32[1536]{0:T(1024)}, u32[]{:S(2)}) copy-start(f32[1536]{0:T(1024)} %param.10) | copy-start | bytes 18436
  19.1 6.6 %copy-start = (f32[256,1536]{1,0:T(8,128)}, f32[256,1536]{1,0:T(8,128)S(1)}, u32[]{:S(2)}) copy-start(f32[256,1536]{1,0:T(8,128)S(1)} %get-tuple-element.74) | copy-start | bytes 4718596
  40.6 17.2 %all-to-all-start = ((f32[4,64,198]{2,1,0:T(8,128)}), f32[4,64,198]{2,1,0:T(8,128)S(1)}, u32[]{:S(2)}, u32[]{:S(2)}) async-start(f32[4,64,198]{2,1,0:T(8,128)} %copy.11), calls=%async_computation | async-start | bytes 524288 | tf_op jit(solution)/shard_map/all_to_all | solution.py:58
  51.0 1.2 %copy-start.1 = (f32[286,1536]{1,0:T(8,128)}, f32[286,1536]{1,0:T(8,128)S(1)}, u32[]{:S(2)}) copy-start(f32[286,1536]{1,0:T(8,128)S(1)} %fusion.1) | copy-start | bytes 5271556
  52.3 41.1 %collective-permute-start.1 = (f32[30,1536]{1,0:T(8,128)S(1)}, f32[30,1536]{1,0:T(8,128)}, u32[]{:S(2)}, u32[]{:S(2)}) collective-permute-start(f32[30,1536]{1,0:T(8,128)S(1)} %slice.581), channel_id=1, source_target_pairs={{2,0},{4,2},{6,4},{8,6},{10,8},{12,10},{14,12},{16,14},{18,16},{20... | collective-permute-start | bytes 552968 | tf_op jit(solution)/shard_map/ppermute | solution.py:22
  58.5 28.8 %all-to-all-start.1 = ((f32[64,1,198]{2,1,0:T(1,128)}), f32[64,1,198]{2,1,0:T(1,128)S(1)}, u32[]{:S(2)}, u32[]{:S(2)}) async-start(f32[64,1,198]{2,1,0:T(1,128)} %all_to_all.19), calls=%async_computation.1 | async-start | bytes 131072 | tf_op jit(solution)/shard_map/all_to_all | solution.py:65
  77.4 31.6 %copy-start.2 = (bf16[256,1536]{1,0:T(8,128)(2,1)S(1)}, bf16[256,1536]{1,0:T(8,128)(2,1)}, u32[]{:S(2)}) copy-start(bf16[256,1536]{1,0:T(8,128)(2,1)} %param.6) | copy-start | bytes 2359300
  77.4 31.6 %copy-start.3 = (bf16[256,1536]{1,0:T(8,128)(2,1)S(1)}, bf16[256,1536]{1,0:T(8,128)(2,1)}, u32[]{:S(2)}) copy-start(bf16[256,1536]{1,0:T(8,128)(2,1)} %param.7) | copy-start | bytes 2359300
  88.0 16.8 %all-to-all-start.2 = ((f32[64,1,198]{2,1,0:T(1,128)}), f32[64,1,198]{2,1,0:T(1,128)S(1)}, u32[]{:S(2)}, u32[]{:S(2)}) async-start(f32[64,1,198]{2,1,0:T(1,128)} %broadcast_in_dim.13), calls=%async_computation.2 | async-start | bytes 131072 | tf_op jit(solution)/shard_map/all_to_all | solution.py:34
  105.6 10.1 %all-to-all-start.3 = ((f32[4,64,198]{2,1,0:T(8,128)}), f32[4,64,198]{2,1,0:T(8,128)S(1)}, u32[]{:S(2)}, u32[]{:S(2)}) async-start(f32[4,64,198]{2,1,0:T(8,128)} %broadcast_in_dim.14), calls=%async_computation.3 | async-start | bytes 524288 | tf_op jit(solution)/shard_map/all_to_all | solution.py:34
where the time goes:
time: 118 us
  starting transfers between devices  38.5 us (33%)
  other arithmetic  32 us (27%)
  waiting for transfers between devices  29.8 us (25%)
  local copies, waits for them, and re-layouts  9.18 us (8%)
  blocking collectives  7.21 us (6%)
  between operations  1.2 us (1%)
    all_to_all x1, starting transfers between devices, sum_by_axis(): return jnp.sum(lax.all_to_all(own, far, 0, 0, tiled=True), axis=0)  17.4 us
    all_to_all x2, waiting for transfers between devices, from_everyone(): return lax.all_to_all(copies, axis, split_axis=0, concat_axis=0, tiled=True)  15.3 us
    all_to_all x1, waiting for transfers between devices, sum_by_axis(): return jnp.sum(lax.all_to_all(own, far, 0, 0, tiled=True), axis=0)  9.85 us
    reduce_sum x5, other arithmetic, body(): jnp.sum(dconv * glu_all[j:j + rows].astype(jnp.float32), axis=0)  9.23 us
    ppermute x2, starting transfers between devices, from_behind(): return lax.ppermute(x, axis, pairs)  8.9 us
    all_to_all x2, starting transfers between devices, from_everyone(): return lax.all_to_all(copies, axis, split_axis=0, concat_axis=0, tiled=True)  8.75 us
    reduce_sum x1, other arithmetic, norm_backward(): mean = total_of_pieces(jnp.sum(conv, axis=1, keepdims=True), 'tp') / D  7.97 us
    all_gather x4, blocking collectives, total_of_pieces(): blocks = lax.all_gather(x, axis)  7.21 us
  transfers between devices with their start and end apart: 6, of which 4 were waited for; matrix products, arithmetic and copies ran while one was open for 11% of the time, Pallas kernels for 0%

commit v1 on v0

v1 whole, which is shorter than its diff:
```python
import functools

import jax
import jax.numpy as jnp
from jax import lax
from jax.experimental import pallas as pl
from jax.experimental.pallas import tpu as pltpu
from jax.sharding import Mesh
from jax.sharding import PartitionSpec as P

SP = ("sp_0", "sp_1", "sp_2")
EPS = 1e-05
F32 = jnp.float32
BF16 = jnp.bfloat16
MESH = pl.DeviceIdType.MESH
S = 16
LANES = 128
ROWS = 256
EDGE = 30
TAPS = 31


def sigmoid(x):
    return 0.5 * jnp.tanh(0.5 * x) + 0.5


def kernel(
    sizes,
    a_hbm,
    g_hbm,
    cot_hbm,
    taps_ref,
    gain_ref,
    shift_ref,
    ag_hbm,
    gg_hbm,
    tg_ref,
    gng_ref,
    shg_ref,
    a_in,
    g_in,
    cot_in,
    a_tail,
    g_tail,
    ap,
    sg,
    cotp,
    ext,
    dce,
    tapb,
    convs,
    dnorm,
    rowsum,
    rowdot,
    mean_l,
    rstd_s,
    m1_s,
    m2_s,
    stat_snd,
    stat_rcv,
    sums_snd,
    sums_rcv,
    halo_snd,
    halo_rcv,
    halo_f,
    back_f,
    back_snd,
    back_rcv,
    col,
    red,
    part,
    part_rcv,
    line_snd,
    line_rcv,
    full_snd,
    full_rcv,
    ag_out,
    gg_out,
    in_sem,
    out_sem,
    tp_send,
    tp_recv,
    halo_send,
    halo_recv,
    red_send,
    red_recv,
):
    nz, ny, nx = sizes
    blocks = ext.shape[0]
    chans = blocks * LANES
    plane = nz * ny
    z, y, x, core = (lax.axis_index(name) for name in (*SP, "tp"))
    sp = (z * ny + y) * nx + x
    total = plane * nx

    def place(index):
        return (index // (ny * nx), index // nx % ny, index % nx, core)

    after = place(lax.rem(sp + 1, total))
    behind = place(lax.rem(sp + total - 1, total))
    other = (z, y, x, 1 - core)
    mine = z * ny + y

    def in_plane(j):
        pz = lax.rem(z + j // ny, nz)
        py = lax.rem(y + j % ny, ny)
        return pz * ny + py, (pz, py, x, core)

    def in_line(j):
        return (z, y, lax.rem(x + j, nx), core)

    tail = pl.ds(ROWS - 32, 32)
    loads = [
        pltpu.make_async_copy(a_hbm.at[tail], a_tail, in_sem.at[0]),
        pltpu.make_async_copy(g_hbm.at[tail], g_tail, in_sem.at[1]),
        pltpu.make_async_copy(a_hbm, a_in, in_sem.at[2]),
        pltpu.make_async_copy(g_hbm, g_in, in_sem.at[3]),
        pltpu.make_async_copy(cot_hbm, cot_in, in_sem.at[4]),
    ]
    for load in loads:
        load.start()

    barrier = pltpu.get_barrier_semaphore()

    def greet(device):
        pl.semaphore_signal(barrier, inc=1, device_id=device, device_id_type=MESH)

    greet(other)
    greet(after)
    greet(behind)

    @pl.loop(1, nx)
    def _(j):
        greet(in_line(j))

    @pl.loop(1, plane)
    def _(j):
        greet(in_plane(j)[1])

    loads[0].wait()
    loads[1].wait()
    for c in range(blocks):
        lanes = pl.ds(c * LANES, LANES)
        halo_snd[c] = (a_tail[:, lanes].astype(F32) * sigmoid(g_tail[:, lanes].astype(F32))).astype(BF16)

    pl.semaphore_wait(barrier, 3 + (nx - 1) + (plane - 1))
    halo = pltpu.make_async_remote_copy(
        halo_snd, halo_rcv, halo_send.at[0], halo_recv.at[0], device_id=after, device_id_type=MESH
    )
    halo.start()

    for c in range(blocks):
        rows = taps_ref[:, c * LANES : (c + 1) * LANES].astype(F32)
        for k in range(TAPS):
            tapb[c, k] = jnp.broadcast_to(rows[k : k + 1], (S, LANES)).astype(BF16)

    at = lax.broadcasted_iota(jnp.int32, (ROWS, ROWS), 0)
    pos = lax.broadcasted_iota(jnp.int32, (ROWS, ROWS), 1)
    perm = jnp.where(pos == (at % S) * S + at // S, 1.0, 0.0).astype(BF16)
    loads[2].wait()
    loads[3].wait()
    loads[4].wait()

    def moved(v):
        return jnp.dot(perm, v, preferred_element_type=F32)

    @pl.loop(0, blocks // 2)
    def _(cc):
        wide = pl.ds(pl.multiple_of(cc * 2 * LANES, 2 * LANES), 2 * LANES)
        av = moved(a_in[:, wide])
        sv = sigmoid(moved(g_in[:, wide]))
        glu = (av * sv).astype(BF16)
        cv = moved(cot_in[:, wide])
        for h in range(2):
            lanes = slice(h * LANES, (h + 1) * LANES)
            c = cc * 2 + h
            ap[c] = av[:, lanes].astype(BF16)
            sg[c] = sv[:, lanes]
            cotp[c] = cv[:, lanes].astype(BF16)
            for r in range(S):
                ext[c, EDGE + r] = glu[r * S : (r + 1) * S, lanes]

    halo.wait_recv()
    row = lax.broadcasted_iota(jnp.int32, (S, LANES), 0)

    @pl.loop(0, blocks)
    def _(c):
        halo_f[c] = jnp.where(sp > 0, halo_rcv[c].astype(F32), 0.0)

    @pl.loop(0, blocks)
    def _(c):
        for r in range(S):
            v = ext[c, EDGE + r].astype(F32)
            one = jnp.where(row == 0, halo_f[c, S + r : S + r + 1], pltpu.roll(v, 1, 0))
            ext[c, EDGE - S + r] = one.astype(BF16)
            if r >= 2:
                two = jnp.where(row == 0, halo_f[c, r : r + 1], pltpu.roll(one, 1, 0))
                ext[c, r - 2] = two.astype(BF16)

    rowsum[...] = jnp.zeros_like(rowsum)

    @pl.loop(0, blocks)
    def _(c):
        for q in range(S // 4):
            acc = [None] * 4
            for k in range(TAPS):
                tap = tapb[c, k].astype(F32)
                for i in range(4):
                    v = ext[c, q * 4 + i + k].astype(F32) * tap
                    acc[i] = v if acc[i] is None else acc[i] + v
            for i in range(4):
                convs[c, q * 4 + i] = acc[i]
                rowsum[q * 4 + i] += acc[i]

    for r in range(S):
        mean_l[r] = jnp.broadcast_to(jnp.sum(rowsum[r], axis=1, keepdims=True) / chans, (S, LANES))

    @pl.loop(0, S)
    def _(r):
        m = mean_l[r]
        acc = jnp.zeros((S, LANES), F32)
        for c in range(blocks):
            cent = convs[c, r] - m
            acc = acc + cent * cent
        rowdot[r] = acc

    lane = lax.broadcasted_iota(jnp.int32, (S, LANES), 1)
    for r in range(S):
        stat_snd[r] = jnp.where(lane == 0, mean_l[r], jnp.sum(rowdot[r], axis=1, keepdims=True))
    stat = pltpu.make_async_remote_copy(
        stat_snd, stat_rcv, tp_send.at[0], tp_recv.at[0], device_id=other, device_id_type=MESH
    )
    stat.start()
    stat.wait()
    for r in range(S):
        own_m, far_m = mean_l[r], jnp.broadcast_to(stat_rcv[r][:, 0:1], (S, LANES))
        own_q, far_q = stat_snd[r][:, 1:2], stat_rcv[r][:, 1:2]
        diff = own_m - far_m
        spread = (own_q + far_q + diff * diff * (chans / 2)) / (2 * chans)
        mean_l[r] = 0.5 * (own_m + far_m)
        rstd_s[r] = lax.rsqrt(spread + EPS)

    col[...] = jnp.zeros_like(col)

    @pl.loop(0, S)
    def _(r):
        m, rs = mean_l[r], rstd_s[r]
        acc1 = jnp.zeros((S, LANES), F32)
        acc2 = jnp.zeros((S, LANES), F32)
        for c in range(blocks):
            lanes = slice(c * LANES, (c + 1) * LANES)
            normed = (convs[c, r] - m) * rs
            gain = gain_ref[:, lanes]
            pre = normed * gain + shift_ref[:, lanes]
            sig = sigmoid(pre)
            cv = cotp[c, pl.ds(pl.multiple_of(r * S, S), S)].astype(F32)
            dpre = cv * sig * (1.0 + pre * (1.0 - sig))
            dn = dpre * gain
            convs[c, r] = normed
            dnorm[c, r] = dn
            acc1 = acc1 + dn
            acc2 = acc2 + dn * normed
            prod = dpre * normed
            col[c, 0] += prod[:8] + prod[8:]
            col[c, 1] += dpre[:8] + dpre[8:]
        rowsum[r] = acc1
        rowdot[r] = acc2

    for r in range(S):
        sums_snd[r] = jnp.where(
            lane == 0,
            jnp.sum(rowsum[r], axis=1, keepdims=True),
            jnp.sum(rowdot[r], axis=1, keepdims=True),
        )
    sums = pltpu.make_async_remote_copy(
        sums_snd, sums_rcv, tp_send.at[1], tp_recv.at[1], device_id=other, device_id_type=MESH
    )
    sums.start()
    sums.wait()
    for r in range(S):
        both = (sums_snd[r] + sums_rcv[r]) / (2 * chans)
        rs = rstd_s[r]
        m1_s[r] = rs * both[:, 0:1]
        m2_s[r] = rs * both[:, 1:2]

    @pl.loop(0, blocks)
    def _(c):
        for r in range(S):
            d = rstd_s[r] * dnorm[c, r] - m1_s[r] - convs[c, r] * m2_s[r]
            dce[c, r] = d.astype(BF16)
            back_f[c, r : r + 1] = d[0:1]
            back_f[c, S + r : S + r + 1] = d[1:2]
        back_snd[c] = back_f[c].astype(BF16)

    back = pltpu.make_async_remote_copy(
        back_snd, back_rcv, halo_send.at[1], halo_recv.at[1], device_id=behind, device_id_type=MESH
    )
    back.start()

    for extra in range(5 * blocks, part.shape[0]):
        part[extra] = jnp.zeros((8, LANES), BF16)

    @pl.loop(0, blocks)
    def _(c):
        for q in range(8):
            ks = [k for k in range(q * 4, q * 4 + 4) if k < TAPS]
            acc = [None] * len(ks)
            for r in range(S):
                d = dce[c, r].astype(F32)
                for i, k in enumerate(ks):
                    v = ext[c, k + r].astype(F32) * d
                    acc[i] = v if acc[i] is None else acc[i] + v
            for i, k in enumerate(ks):
                red[pl.ds(9 * k, 8), :] = acc[i][:8] + acc[i][8:]
        red[pl.ds(9 * TAPS, 8), :] = col[c, 0]
        for g in range(4):
            rows = red[pl.ds(72 * g, 8, stride=9), :]
            for s in range(1, 8):
                rows = rows + red[pl.ds(72 * g + s, 8, stride=9), :]
            part[5 * c + g] = rows.astype(BF16)
        part[5 * c + 4] = jnp.broadcast_to(jnp.sum(col[c, 1], axis=0, keepdims=True), (8, LANES)).astype(BF16)

    per = part.shape[0] // plane

    def shard(index):
        return pl.ds(index * per, per)

    def scatter(index, device):
        return pltpu.make_async_remote_copy(
            part.at[shard(index)],
            part_rcv.at[shard(mine)],
            red_send.at[0],
            red_recv.at[0],
            device_id=device,
            device_id_type=MESH,
        )

    @pl.loop(1, plane)
    def _(j):
        scatter(*in_plane(j)).start()

    part_rcv[shard(mine)] = part[shard(mine)]

    back.wait_recv()

    @pl.loop(0, blocks)
    def _(c):
        halo_f[c] = jnp.where(sp < total - 1, back_rcv[c].astype(F32), 0.0)

    @pl.loop(0, blocks)
    def _(c):
        for r in range(S):
            v = dce[c, r].astype(F32)
            one = jnp.where(row == S - 1, halo_f[c, r : r + 1], pltpu.roll(v, S - 1, 0))
            dce[c, S + r] = one.astype(BF16)
            if r < EDGE - S:
                two = jnp.where(row == S - 1, halo_f[c, S + r : S + r + 1], pltpu.roll(one, S - 1, 0))
                dce[c, 2 * S + r] = two.astype(BF16)

    @pl.loop(0, blocks)
    def _(c):
        for q in range(S // 4):
            acc = [None] * 4
            for k in range(TAPS):
                tap = tapb[c, k].astype(F32)
                for i in range(4):
                    v = dce[c, q * 4 + i + EDGE - k].astype(F32) * tap
                    acc[i] = v if acc[i] is None else acc[i] + v
            for i in range(4):
                convs[c, q * 4 + i] = acc[i]

    @pl.loop(0, blocks // 2)
    def _(cc):
        wide = pl.ds(pl.multiple_of(cc * 2 * LANES, 2 * LANES), 2 * LANES)
        da, dg = [], []
        for h in range(2):
            c = cc * 2 + h
            grad = convs[c].reshape(ROWS, LANES)
            sv = sg[c]
            first = grad * sv
            da.append(first.astype(BF16))
            dg.append((first * ap[c].astype(F32) * (1.0 - sv)).astype(BF16))
        ag_out[:, wide] = moved(jnp.concatenate(da, axis=1)).astype(BF16)
        gg_out[:, wide] = moved(jnp.concatenate(dg, axis=1)).astype(BF16)

    stores = [
        pltpu.make_async_copy(ag_out, ag_hbm, out_sem.at[0]),
        pltpu.make_async_copy(gg_out, gg_hbm, out_sem.at[1]),
    ]
    for store in stores:
        store.start()

    def wait_all(ref, count, size, sem):
        some = ref.at[pl.ds(0, count * size)]
        pltpu.make_async_copy(some, some, sem).wait()

    wait_all(part_rcv, plane - 1, per, red_recv.at[0])
    sums8 = part_rcv[pl.ds(0, per)].astype(F32)
    for j in range(1, plane):
        sums8 = sums8 + part_rcv[pl.ds(j * per, per)].astype(F32)
    line_snd[...] = sums8
    line_rcv[pl.ds(x * per, per)] = sums8

    def along(j):
        return pltpu.make_async_remote_copy(
            line_snd,
            line_rcv.at[shard(x)],
            red_send.at[1],
            red_recv.at[1],
            device_id=in_line(j),
            device_id_type=MESH,
        )

    @pl.loop(1, nx)
    def _(j):
        along(j).start()

    wait_all(line_rcv, nx - 1, per, red_recv.at[1])
    sums8 = line_rcv[pl.ds(0, per)]
    for j in range(1, nx):
        sums8 = sums8 + line_rcv[pl.ds(j * per, per)]
    full_snd[...] = sums8.astype(BF16)
    full_rcv[shard(mine)] = sums8.astype(BF16)

    def spread_out(j):
        return pltpu.make_async_remote_copy(
            full_snd,
            full_rcv.at[shard(mine)],
            red_send.at[2],
            red_recv.at[2],
            device_id=in_plane(j)[1],
            device_id_type=MESH,
        )

    @pl.loop(1, plane)
    def _(j):
        spread_out(j).start()

    wait_all(full_rcv, plane - 1, per, red_recv.at[2])
    for c in range(blocks):
        lanes = slice(c * LANES, (c + 1) * LANES)
        for g in range(4):
            rows = full_rcv[5 * c + g].astype(F32)
            if g < 3:
                tg_ref[8 * g : 8 * g + 8, lanes] = rows
            else:
                tg_ref[24:TAPS, lanes] = rows[:7]
                gng_ref[:, lanes] = rows[7:8]
        shg_ref[:, lanes] = full_rcv[5 * c + 4].astype(F32)[0:1]

    for store in stores:
        store.wait()
    halo.wait_send()
    back.wait_send()
    wait_all(part, plane - 1, per, red_send.at[0])
    wait_all(line_rcv, nx - 1, per, red_send.at[1])
    wait_all(full_rcv, plane - 1, per, red_send.at[2])


def body(sizes, proj_a, proj_gate, taps, norm_gain, norm_shift, cotangent):
    rows, chans = proj_a.shape
    blocks = chans // LANES
    nz, ny, nx = sizes
    plane = nz * ny
    per = -(-5 * blocks // plane)
    shards = per * plane
    any_space = pl.BlockSpec(memory_space=pl.ANY)
    vmem = pl.BlockSpec(memory_space=pltpu.VMEM)
    tile = (S, S, LANES)
    edge = (blocks, 32, LANES)
    outs = pl.pallas_call(
        functools.partial(kernel, sizes),
        out_shape=(
            jax.ShapeDtypeStruct((rows, chans), BF16),
            jax.ShapeDtypeStruct((rows, chans), BF16),
            jax.ShapeDtypeStruct((TAPS, chans), F32),
            jax.ShapeDtypeStruct((1, chans), F32),
            jax.ShapeDtypeStruct((1, chans), F32),
        ),
        in_specs=[any_space] * 3 + [vmem] * 3,
        out_specs=(any_space, any_space, vmem, vmem, vmem),
        scratch_shapes=[
            pltpu.VMEM((rows, chans), BF16),
            pltpu.VMEM((rows, chans), BF16),
            pltpu.VMEM((rows, chans), BF16),
            pltpu.VMEM((32, chans), BF16),
            pltpu.VMEM((32, chans), BF16),
            pltpu.VMEM((blocks, rows, LANES), BF16),
            pltpu.VMEM((blocks, rows, LANES), F32),
            pltpu.VMEM((blocks, rows, LANES), BF16),
            pltpu.VMEM((blocks, EDGE + S, S, LANES), BF16),
            pltpu.VMEM((blocks, EDGE + S, S, LANES), BF16),
            pltpu.VMEM((blocks, TAPS, S, LANES), BF16),
            pltpu.VMEM((blocks, *tile), F32),
            pltpu.VMEM((blocks, *tile), F32),
            pltpu.VMEM(tile, F32),
            pltpu.VMEM(tile, F32),
            pltpu.VMEM(tile, F32),
            pltpu.VMEM(tile, F32),
            pltpu.VMEM(tile, F32),
            pltpu.VMEM(tile, F32),
            pltpu.VMEM(tile, F32),
            pltpu.VMEM(tile, F32),
            pltpu.VMEM(tile, F32),
            pltpu.VMEM(tile, F32),
            pltpu.VMEM(edge, BF16),
            pltpu.VMEM(edge, BF16),
            pltpu.VMEM(edge, F32),
            pltpu.VMEM(edge, F32),
            pltpu.VMEM(edge, BF16),
            pltpu.VMEM(edge, BF16),
            pltpu.VMEM((blocks, 2, 8, LANES), F32),
            pltpu.VMEM((9 * 32, LANES), F32),
            pltpu.VMEM((shards, 8, LANES), BF16),
            pltpu.VMEM((shards, 8, LANES), BF16),
            pltpu.VMEM((per, 8, LANES), F32),
            pltpu.VMEM((nx * per, 8, LANES), F32),
            pltpu.VMEM((per, 8, LANES), BF16),
            pltpu.VMEM((shards, 8, LANES), BF16),
            pltpu.VMEM((rows, chans), BF16),
            pltpu.VMEM((rows, chans), BF16),
            pltpu.SemaphoreType.DMA((5,)),
            pltpu.SemaphoreType.DMA((2,)),
            pltpu.SemaphoreType.DMA((2,)),
            pltpu.SemaphoreType.DMA((2,)),
            pltpu.SemaphoreType.DMA((2,)),
            pltpu.SemaphoreType.DMA((2,)),
            pltpu.SemaphoreType.DMA((3,)),
            pltpu.SemaphoreType.DMA((3,)),
        ],
        compiler_params=pltpu.CompilerParams(
            collective_id=0, has_side_effects=True, vmem_limit_bytes=48 * 1024 * 1024
        ),
    )(proj_a, proj_gate, cotangent, taps, norm_gain.reshape(1, -1), norm_shift.reshape(1, -1))
    a_grad, gate_grad, taps_grad, gain_grad, shift_grad = outs
    return (a_grad, gate_grad, taps_grad, gain_grad.reshape(-1), shift_grad.reshape(-1))


def solution(mesh):
    sizes = (8, 8, 4)
    torus = Mesh(mesh.devices.reshape(*sizes, mesh.shape["tp"]), (*SP, "tp"))
    return jax.shard_map(
        functools.partial(body, sizes),
        mesh=torus,
        in_specs=(P(SP, "tp"), P(SP, "tp"), P(None, "tp"), P("tp"), P("tp"), P(SP, "tp")),
        out_specs=(P(SP, "tp"), P(SP, "tp"), P(None, "tp"), P("tp"), P("tp")),
        check_vma=False,
    )
```

time: 118 us -> 60.9 us (0.52)
  Pallas kernels: 0 us -> 51.3 us
  starting transfers between devices: 38.5 us -> 0 us
  other arithmetic: 32 us -> 1.24 us
  waiting for transfers between devices: 29.8 us -> 0 us
  blocking collectives: 7.21 us -> 0 us
  local copies, waits for them, and re-layouts: 9.18 us -> 7.44 us
    pallas_call x0 -> x1, Pallas kernels: none -> 51.3 us  [body(): pl.pallas_call(functools.partial(kernel, sizes), out_shape=(jax.ShapeDtyp...]
    all_to_all x4 -> x0, starting transfers between devices: 29.6 us -> none  [the longest x1 17.4 us: sum_by_axis(): return jnp.sum(lax.all_to_all(own, far, 0, 0, tiled=True), axis=0)]
    all_to_all x4 -> x0, waiting for transfers between devices: 25.1 us -> none  [the longest x2 15.3 us: from_everyone(): return lax.all_to_all(copies, axis, split_axis=0, concat_axis=0, tiled=True)]
    reduce_sum x14 -> x0, other arithmetic: 20.2 us -> none  [the longest x5 9.23 us: body(): jnp.sum(dconv * glu_all[j:j + rows].astype(jnp.float32), axis=0)]
    ppermute x2 -> x0, starting transfers between devices: 8.9 us -> none  [from_behind(): return lax.ppermute(x, axis, pairs)]
    add x2 -> x0, other arithmetic: 7.81 us -> none  [the longest x1 6.76 us: transposed(): total = total + tapf[edge - k] * source[k:k + count]]
    all_gather x4 -> x0, blocking collectives: 7.21 us -> none  [total_of_pieces(): blocks = lax.all_gather(x, axis)]
    unnamed x17 -> x13, local copies, waits for them, and re-layouts: 1.25 us -> 6.72 us
  transfers between devices with their start and end apart: 6 -> 0, of which waited for: 4 -> 0; matrix products, arithmetic and copies ran while one was open for 11% -> 0% of each run, Pallas kernels for 0% -> 0%
where the time goes in v1:
time: 60.9 us; the launch traced here: 60.6 us
  Pallas kernels  51.3 us (84%)
  local copies, waits for them, and re-layouts  7.44 us (12%)
  other arithmetic  1.24 us (2%)
  between operations  0.67 us (1%)
    pallas_call x1, Pallas kernels, body(): pl.pallas_call(functools.partial(kernel, sizes), out_shape=(jax.ShapeDtyp...  51.3 us
    unnamed x13, local copies, waits for them, and re-layouts  6.72 us
    pallas_call x2, other arithmetic, body(): pl.pallas_call(functools.partial(kernel, sizes), out_shape=(jax.ShapeDtyp...  1.24 us

profile of v1, /device:TPU:8, one launch (start us, length us, event | category | flops | bytes accessed | tf_op | source)
XLA Modules:
  0.0 60.6 jit_solution(11980830347095414697)
XLA Ops:
  0.6 0.0 copy-start.4
  0.6 0.7 %reshape.22.gain_ref = f32[1,1536]{1,0:T(1,128)S(1)} reshape(f32[1536]{0:T(1024)} %param.9) | data formatting | bytes 12288 | tf_op jit(solution)/shard_map/reshape | solution.py:534
  1.3 0.0 copy-done.4
  1.4 0.0 copy-start
  1.4 1.1 %copy-done = bf16[256,1536]{1,0:T(8,128)(2,1)S(1)} copy-done((bf16[256,1536]{1,0:T(8,128)(2,1)S(1)}, bf16[256,1536]{1,0:T(8,128)(2,1)}, u32[]{:S(2)}) %copy-start) | copy-done | bytes 786456
  2.5 0.0 copy-start.1
  2.5 1.1 %copy-done.1 = bf16[256,1536]{1,0:T(8,128)(2,1)S(1)} copy-done((bf16[256,1536]{1,0:T(8,128)(2,1)S(1)}, bf16[256,1536]{1,0:T(8,128)(2,1)}, u32[]{:S(2)}) %copy-start.1) | copy-done | bytes 786456
  3.6 0.0 copy-start.2
  3.6 1.1 %copy-done.2 = bf16[256,1536]{1,0:T(8,128)(2,1)S(1)} copy-done((bf16[256,1536]{1,0:T(8,128)(2,1)S(1)}, bf16[256,1536]{1,0:T(8,128)(2,1)}, u32[]{:S(2)}) %copy-start.2) | copy-done | bytes 786456
  4.8 0.0 copy-start.3
  4.8 0.9 %copy-done.3 = bf16[31,1536]{1,0:T(8,128)(2,1)S(1)} copy-done((bf16[31,1536]{1,0:T(8,128)(2,1)S(1)}, bf16[31,1536]{1,0:T(8,128)(2,1)}, u32[]{:S(2)}) %copy-start.3) | copy-done | bytes 95256
  5.7 51.3 %shard_map.101 = (bf16[256,1536]{1,0:T(8,128)(2,1)S(1)}, bf16[256,1536]{1,0:T(8,128)(2,1)S(1)}, f32[31,1536]{1,0:T(8,128)S(1)}, f32[1,1536]{1,0:T(1,128)S(1)}, f32[1,1536]{1,0:T(1,128)S(1)}) custom-call(bf16[256,1536]{1,0:T(8,128)(2,1)S(1)} %copy-done, bf16[256,1536]{1,0:T(8,128)(2,1)S(1)} %copy-done.1, bf16[256,1536]{1,0:T(8,128)(2,1)S(1)} %copy-done.2, ...), custom_call_target="tpu_custom_call" | custom-call | tf_op jit(solution)/shard_map/pallas_call | solution.py:471
  57.0 0.6 %reduce = f32[1536]{0:T(1024)} reduce(f32[1,1536]{1,0:T(1,128)S(1)} %get-tuple-element.13, f32[]{:T(128)} %constant), dimensions={0}, to_apply=%get-tuple-element.13.reduce_sub_computation | reduce | bytes 12292 | tf_op jit(solution)/shard_map/pallas_call | solution.py:471
  57.6 0.6 %reduce.1 = f32[1536]{0:T(1024)} reduce(f32[1,1536]{1,0:T(1,128)S(1)} %get-tuple-element.14, f32[]{:T(128)} %constant), dimensions={0}, to_apply=%get-tuple-element.14.reduce_sub_computation | reduce | bytes 12292 | tf_op jit(solution)/shard_map/pallas_call | solution.py:471
  58.2 0.9 %copy.14 = bf16[256,1536]{1,0:T(8,128)(2,1)} copy(bf16[256,1536]{1,0:T(8,128)(2,1)S(1)} %get-tuple-element.20) | data formatting | bytes 1572864
  59.1 0.9 %copy.15 = bf16[256,1536]{1,0:T(8,128)(2,1)} copy(bf16[256,1536]{1,0:T(8,128)(2,1)S(1)} %get-tuple-element.21) | data formatting | bytes 1572864
  60.0 0.7 %copy.16 = f32[31,1536]{1,0:T(8,128)} copy(f32[31,1536]{1,0:T(8,128)S(1)} %get-tuple-element.22) | data formatting | bytes 380928
  (1 shorter events, 0.0 us)
Async XLA Ops:
  0.6 0.7 %copy-start.4 = (f32[1536]{0:T(1024)S(1)}, f32[1536]{0:T(1024)}, u32[]{:S(2)}) copy-start(f32[1536]{0:T(1024)} %param.10) | copy-start | bytes 18436
  1.4 1.1 %copy-start = (bf16[256,1536]{1,0:T(8,128)(2,1)S(1)}, bf16[256,1536]{1,0:T(8,128)(2,1)}, u32[]{:S(2)}) copy-start(bf16[256,1536]{1,0:T(8,128)(2,1)} %a_hbm.1) | copy-start | bytes 2359300
  2.5 1.1 %copy-start.1 = (bf16[256,1536]{1,0:T(8,128)(2,1)S(1)}, bf16[256,1536]{1,0:T(8,128)(2,1)}, u32[]{:S(2)}) copy-start(bf16[256,1536]{1,0:T(8,128)(2,1)} %g_hbm.1) | copy-start | bytes 2359300
  3.6 1.1 %copy-start.2 = (bf16[256,1536]{1,0:T(8,128)(2,1)S(1)}, bf16[256,1536]{1,0:T(8,128)(2,1)}, u32[]{:S(2)}) copy-start(bf16[256,1536]{1,0:T(8,128)(2,1)} %cot_hbm.1) | copy-start | bytes 2359300
  4.8 0.9 %copy-start.3 = (bf16[31,1536]{1,0:T(8,128)(2,1)S(1)}, bf16[31,1536]{1,0:T(8,128)(2,1)}, u32[]{:S(2)}) copy-start(bf16[31,1536]{1,0:T(8,128)(2,1)} %taps_ref.1) | copy-start | bytes 285700

commit v2 on v1

--- a/solution.py
+++ b/solution.py
@@ -29,11 +29,11 @@
     a_hbm,
     g_hbm,
     cot_hbm,
-    taps_ref,
-    gain_ref,
-    shift_ref,
-    ag_hbm,
-    gg_hbm,
+    taps_hbm,
+    gain_hbm,
+    shift_hbm,
+    ag_out,
+    gg_out,
     tg_ref,
     gng_ref,
     shg_ref,
@@ -74,10 +74,10 @@
     line_rcv,
     full_snd,
     full_rcv,
-    ag_out,
-    gg_out,
+    gain_ref,
+    shift_ref,
+    taps_in,
     in_sem,
-    out_sem,
     tp_send,
     tp_recv,
     halo_send,
@@ -101,13 +101,17 @@
     other = (z, y, x, 1 - core)
     mine = z * ny + y
 
-    def in_plane(j):
-        pz = lax.rem(z + j // ny, nz)
-        py = lax.rem(y + j % ny, ny)
-        return pz * ny + py, (pz, py, x, core)
-
-    def in_line(j):
-        return (z, y, lax.rem(x + j, nx), core)
+    zs = [lax.rem(z + j, nz) for j in range(nz)]
+    ys = [lax.rem(y + j, ny) for j in range(ny)]
+    line = [(z, y, lax.rem(x + j, nx), core) for j in range(1, nx)]
+
+    def far(n, j):
+        return min(j, n - j)
+
+    steps = sorted(
+        ((j, i) for j in range(nz) for i in range(ny) if (j, i) != (0, 0)), key=lambda v: -far(nz, v[0]) - far(ny, v[1])
+    )
+    others = [(zs[j] * ny + ys[i], (zs[j], ys[i], x, core)) for j, i in steps]
 
     tail = pl.ds(ROWS - 32, 32)
     loads = [
@@ -115,7 +119,10 @@
         pltpu.make_async_copy(g_hbm.at[tail], g_tail, in_sem.at[1]),
         pltpu.make_async_copy(a_hbm, a_in, in_sem.at[2]),
         pltpu.make_async_copy(g_hbm, g_in, in_sem.at[3]),
-        pltpu.make_async_copy(cot_hbm, cot_in, in_sem.at[4]),
+        pltpu.make_async_copy(taps_hbm, taps_in, in_sem.at[4]),
+        pltpu.make_async_copy(cot_hbm, cot_in, in_sem.at[5]),
+        pltpu.make_async_copy(gain_hbm, gain_ref, in_sem.at[6]),
+        pltpu.make_async_copy(shift_hbm, shift_ref, in_sem.at[7]),
     ]
     for load in loads:
         load.start()
@@ -129,13 +136,10 @@
     greet(after)
     greet(behind)
 
-    @pl.loop(1, nx)
-    def _(j):
-        greet(in_line(j))
-
-    @pl.loop(1, plane)
-    def _(j):
-        greet(in_plane(j)[1])
+    for device in line:
+        greet(device)
+    for _, device in others:
+        greet(device)
 
     loads[0].wait()
     loads[1].wait()
@@ -143,23 +147,17 @@
         lanes = pl.ds(c * LANES, LANES)
         halo_snd[c] = (a_tail[:, lanes].astype(F32) * sigmoid(g_tail[:, lanes].astype(F32))).astype(BF16)
 
-    pl.semaphore_wait(barrier, 3 + (nx - 1) + (plane - 1))
-    halo = pltpu.make_async_remote_copy(
-        halo_snd, halo_rcv, halo_send.at[0], halo_recv.at[0], device_id=after, device_id_type=MESH
-    )
-    halo.start()
-
+    loads[4].wait()
     for c in range(blocks):
-        rows = taps_ref[:, c * LANES : (c + 1) * LANES].astype(F32)
+        rows = taps_in[:, c * LANES : (c + 1) * LANES].astype(F32)
         for k in range(TAPS):
             tapb[c, k] = jnp.broadcast_to(rows[k : k + 1], (S, LANES)).astype(BF16)
 
     at = lax.broadcasted_iota(jnp.int32, (ROWS, ROWS), 0)
     pos = lax.broadcasted_iota(jnp.int32, (ROWS, ROWS), 1)
     perm = jnp.where(pos == (at % S) * S + at // S, 1.0, 0.0).astype(BF16)
-    loads[2].wait()
-    loads[3].wait()
-    loads[4].wait()
+    for i in (2, 3, 5, 6, 7):
+        loads[i].wait()
 
     def moved(v):
         return jnp.dot(perm, v, preferred_element_type=F32)
@@ -180,6 +178,11 @@
             for r in range(S):
                 ext[c, EDGE + r] = glu[r * S : (r + 1) * S, lanes]
 
+    pl.semaphore_wait(barrier, 3 + (nx - 1) + (plane - 1))
+    halo = pltpu.make_async_remote_copy(
+        halo_snd, halo_rcv, halo_send.at[0], halo_recv.at[0], device_id=after, device_id_type=MESH
+    )
+    halo.start()
     halo.wait_recv()
     row = lax.broadcasted_iota(jnp.int32, (S, LANES), 0)
 
@@ -250,8 +253,8 @@
         for c in range(blocks):
             lanes = slice(c * LANES, (c + 1) * LANES)
             normed = (convs[c, r] - m) * rs
-            gain = gain_ref[:, lanes]
-            pre = normed * gain + shift_ref[:, lanes]
+            gain = gain_ref[lanes].reshape(1, LANES)
+            pre = normed * gain + shift_ref[lanes].reshape(1, LANES)
             sig = sigmoid(pre)
             cv = cotp[c, pl.ds(pl.multiple_of(r * S, S), S)].astype(F32)
             dpre = cv * sig * (1.0 + pre * (1.0 - sig))
@@ -335,9 +338,8 @@
             device_id_type=MESH,
         )
 
-    @pl.loop(1, plane)
-    def _(j):
-        scatter(*in_plane(j)).start()
+    for index, device in others:
+        scatter(index, device).start()
 
     part_rcv[shard(mine)] = part[shard(mine)]
 
@@ -383,13 +385,6 @@
         ag_out[:, wide] = moved(jnp.concatenate(da, axis=1)).astype(BF16)
         gg_out[:, wide] = moved(jnp.concatenate(dg, axis=1)).astype(BF16)
 
-    stores = [
-        pltpu.make_async_copy(ag_out, ag_hbm, out_sem.at[0]),
-        pltpu.make_async_copy(gg_out, gg_hbm, out_sem.at[1]),
-    ]
-    for store in stores:
-        store.start()
-
     def wait_all(ref, count, size, sem):
         some = ref.at[pl.ds(0, count * size)]
         pltpu.make_async_copy(some, some, sem).wait()
@@ -401,19 +396,15 @@
     line_snd[...] = sums8
     line_rcv[pl.ds(x * per, per)] = sums8
 
-    def along(j):
-        return pltpu.make_async_remote_copy(
+    for device in line:
+        pltpu.make_async_remote_copy(
             line_snd,
             line_rcv.at[shard(x)],
             red_send.at[1],
             red_recv.at[1],
-            device_id=in_line(j),
+            device_id=device,
             device_id_type=MESH,
-        )
-
-    @pl.loop(1, nx)
-    def _(j):
-        along(j).start()
+        ).start()
 
     wait_all(line_rcv, nx - 1, per, red_recv.at[1])
     sums8 = line_rcv[pl.ds(0, per)]
@@ -422,19 +413,15 @@
     full_snd[...] = sums8.astype(BF16)
     full_rcv[shard(mine)] = sums8.astype(BF16)
 
-    def spread_out(j):
-        return pltpu.make_async_remote_copy(
+    for _, device in others:
+        pltpu.make_async_remote_copy(
             full_snd,
             full_rcv.at[shard(mine)],
             red_send.at[2],
             red_recv.at[2],
-            device_id=in_plane(j)[1],
+            device_id=device,
             device_id_type=MESH,
-        )
-
-    @pl.loop(1, plane)
-    def _(j):
-        spread_out(j).start()
+        ).start()
 
     wait_all(full_rcv, plane - 1, per, red_recv.at[2])
     for c in range(blocks):
@@ -445,16 +432,24 @@
                 tg_ref[8 * g : 8 * g + 8, lanes] = rows
             else:
                 tg_ref[24:TAPS, lanes] = rows[:7]
-                gng_ref[:, lanes] = rows[7:8]
-        shg_ref[:, lanes] = full_rcv[5 * c + 4].astype(F32)[0:1]
-
-    for store in stores:
-        store.wait()
+                gng_ref[lanes] = rows[7:8].reshape(LANES)
+        shg_ref[lanes] = full_rcv[5 * c + 4].astype(F32)[0:1].reshape(LANES)
+
     halo.wait_send()
     back.wait_send()
     wait_all(part, plane - 1, per, red_send.at[0])
     wait_all(line_rcv, nx - 1, per, red_send.at[1])
     wait_all(full_rcv, plane - 1, per, red_send.at[2])
+
+
+def put_out(*refs):
+    count = len(refs) // 2
+    sem = refs[-1]
+    copies = [pltpu.make_async_copy(refs[i], refs[count + i], sem.at[i]) for i in range(count)]
+    for copy in copies:
+        copy.start()
+    for copy in copies:
+        copy.wait()
 
 
 def body(sizes, proj_a, proj_gate, taps, norm_gain, norm_shift, cotangent):
@@ -464,21 +459,22 @@
     plane = nz * ny
     per = -(-5 * blocks // plane)
     shards = per * plane
-    any_space = pl.BlockSpec(memory_space=pl.ANY)
+    hbm = pl.BlockSpec(memory_space=pltpu.HBM)
     vmem = pl.BlockSpec(memory_space=pltpu.VMEM)
     tile = (S, S, LANES)
     edge = (blocks, 32, LANES)
+    shapes = (
+        jax.ShapeDtypeStruct((rows, chans), BF16),
+        jax.ShapeDtypeStruct((rows, chans), BF16),
+        jax.ShapeDtypeStruct((TAPS, chans), F32),
+        jax.ShapeDtypeStruct((chans,), F32),
+        jax.ShapeDtypeStruct((chans,), F32),
+    )
     outs = pl.pallas_call(
         functools.partial(kernel, sizes),
-        out_shape=(
-            jax.ShapeDtypeStruct((rows, chans), BF16),
-            jax.ShapeDtypeStruct((rows, chans), BF16),
-            jax.ShapeDtypeStruct((TAPS, chans), F32),
-            jax.ShapeDtypeStruct((1, chans), F32),
-            jax.ShapeDtypeStruct((1, chans), F32),
-        ),
-        in_specs=[any_space] * 3 + [vmem] * 3,
-        out_specs=(any_space, any_space, vmem, vmem, vmem),
+        out_shape=shapes,
+        in_specs=[hbm] * 6,
+        out_specs=(vmem,) * 5,
         scratch_shapes=[
             pltpu.VMEM((rows, chans), BF16),
             pltpu.VMEM((rows, chans), BF16),
@@ -517,10 +513,10 @@
             pltpu.VMEM((nx * per, 8, LANES), F32),
             pltpu.VMEM((per, 8, LANES), BF16),
             pltpu.VMEM((shards, 8, LANES), BF16),
-            pltpu.VMEM((rows, chans), BF16),
-            pltpu.VMEM((rows, chans), BF16),
-            pltpu.SemaphoreType.DMA((5,)),
-            pltpu.SemaphoreType.DMA((2,)),
+            pltpu.VMEM((chans,), F32),
+            pltpu.VMEM((chans,), F32),
+            pltpu.VMEM((TAPS, chans), BF16),
+            pltpu.SemaphoreType.DMA((8,)),
             pltpu.SemaphoreType.DMA((2,)),
             pltpu.SemaphoreType.DMA((2,)),
             pltpu.SemaphoreType.DMA((2,)),
@@ -529,11 +525,17 @@
             pltpu.SemaphoreType.DMA((3,)),
         ],
         compiler_params=pltpu.CompilerParams(
-            collective_id=0, has_side_effects=True, vmem_limit_bytes=48 * 1024 * 1024
+            collective_id=0, has_side_effects=True, vmem_limit_bytes=50_000_000
         ),
-    )(proj_a, proj_gate, cotangent, taps, norm_gain.reshape(1, -1), norm_shift.reshape(1, -1))
-    a_grad, gate_grad, taps_grad, gain_grad, shift_grad = outs
-    return (a_grad, gate_grad, taps_grad, gain_grad.reshape(-1), shift_grad.reshape(-1))
+    )(proj_a, proj_gate, cotangent, taps, norm_gain, norm_shift)
+    return pl.pallas_call(
+        put_out,
+        out_shape=shapes,
+        in_specs=[vmem] * 5,
+        out_specs=(hbm,) * 5,
+        scratch_shapes=[pltpu.SemaphoreType.DMA((5,))],
+        compiler_params=pltpu.CompilerParams(vmem_limit_bytes=16 * 1024 * 1024),
+    )(*outs)
 
 
 def solution(mesh):

time: 60.9 us -> 58.3 us (0.957)
  local copies, waits for them, and re-layouts: 7.44 us -> 5.68 us
  other arithmetic: 1.24 us -> 0 us
    pallas_call x2 -> x0, other arithmetic: 1.24 us -> none  [body(): pl.pallas_call(functools.partial(kernel, sizes), out_shape=(jax.ShapeDtyp...]
    unnamed x13 -> x12, local copies, waits for them, and re-layouts: 6.72 us -> 5.68 us
    reshape x2 -> x0, local copies, waits for them, and re-layouts: 0.71 us -> none  [the longest x1 0.71 us: body(): norm_gain.reshape(1, -1)]
    pallas_call x1 -> x2, Pallas kernels: 51.3 us -> 51.6 us  [the longest x1 50.4 us: body(): pl.pallas_call(functools.partial(kernel, sizes), out_shape=shapes, in_spe...]
where the time goes in v2:
time: 58.3 us; the launch traced here: 57.9 us
  Pallas kernels  51.6 us (89%)
  local copies, waits for them, and re-layouts  5.68 us (10%)
  between operations  0.65 us (1%)
    pallas_call x1, Pallas kernels, body(): pl.pallas_call(functools.partial(kernel, sizes), out_shape=shapes, in_spe...  50.4 us
    unnamed x12, local copies, waits for them, and re-layouts  5.68 us
    pallas_call x1, Pallas kernels, body(): pl.pallas_call(put_out, out_shape=shapes, in_specs=[vmem] * 5, out_specs=...  1.25 us

profile of v2, /device:TPU:8, one launch (start us, length us, event | category | flops | bytes accessed | tf_op | source)
XLA Modules:
  0.0 57.9 jit_solution(3627099318468542489)
XLA Ops:
  0.6 0.0 copy-start
  0.6 1.1 %copy-done = bf16[256,1536]{1,0:T(8,128)(2,1)S(1)} copy-done((bf16[256,1536]{1,0:T(8,128)(2,1)S(1)}, bf16[256,1536]{1,0:T(8,128)(2,1)}, u32[]{:S(2)}) %copy-start) | copy-done | bytes 786456
  1.8 0.0 copy-start.1
  1.8 1.1 %copy-done.1 = bf16[256,1536]{1,0:T(8,128)(2,1)S(1)} copy-done((bf16[256,1536]{1,0:T(8,128)(2,1)S(1)}, bf16[256,1536]{1,0:T(8,128)(2,1)}, u32[]{:S(2)}) %copy-start.1) | copy-done | bytes 786456
  2.9 0.0 copy-start.2
  2.9 1.1 %copy-done.2 = bf16[256,1536]{1,0:T(8,128)(2,1)S(1)} copy-done((bf16[256,1536]{1,0:T(8,128)(2,1)S(1)}, bf16[256,1536]{1,0:T(8,128)(2,1)}, u32[]{:S(2)}) %copy-start.2) | copy-done | bytes 786456
  4.0 0.0 copy-start.3
  4.0 0.9 %copy-done.3 = bf16[31,1536]{1,0:T(8,128)(2,1)S(1)} copy-done((bf16[31,1536]{1,0:T(8,128)(2,1)S(1)}, bf16[31,1536]{1,0:T(8,128)(2,1)}, u32[]{:S(2)}) %copy-start.3) | copy-done | bytes 95256
  4.9 0.0 copy-start.4
  4.9 0.7 %copy-done.4 = f32[1536]{0:T(1024)S(1)} copy-done((f32[1536]{0:T(1024)S(1)}, f32[1536]{0:T(1024)}, u32[]{:S(2)}) %copy-start.4) | copy-done | bytes 6168
  5.6 0.0 copy-start.5
  5.6 0.7 %copy-done.5 = f32[1536]{0:T(1024)S(1)} copy-done((f32[1536]{0:T(1024)S(1)}, f32[1536]{0:T(1024)}, u32[]{:S(2)}) %copy-start.5) | copy-done | bytes 6168
  6.3 50.4 %shard_map.101 = (bf16[256,1536]{1,0:T(8,128)(2,1)S(1)}, bf16[256,1536]{1,0:T(8,128)(2,1)S(1)}, f32[31,1536]{1,0:T(8,128)S(1)}, f32[1536]{0:T(1024)S(1)}, f32[1536]{0:T(1024)S(1)}) custom-call(bf16[256,1536]{1,0:T(8,128)(2,1)S(1)} %copy-done, bf16[256,1536]{1,0:T(8,128)(2,1)S(1)} %copy-done.1, bf16[256,1536]{1,0:T(8,128)(2,1)S(1)} %copy-done.2, ...), custom_call_target="tpu_custom_call" | custom-call | tf_op jit(solution)/shard_map/pallas_call | solution.py:473
  56.7 1.2 %shard_map.102 = (bf16[256,1536]{1,0:T(8,128)(2,1)}, bf16[256,1536]{1,0:T(8,128)(2,1)}, f32[31,1536]{1,0:T(8,128)}, f32[1536]{0:T(1024)}, f32[1536]{0:T(1024)}) custom-call(bf16[256,1536]{1,0:T(8,128)(2,1)S(1)} %get-tuple-element.10.refs_0_, bf16[256,1536]{1,0:T(8,128)(2,1)S(1)} %get-tuple-element.11.refs_1_, f32[31,1536]{1,0:T(8,128)S(1)} %get-tuple-element.12.refs_2_, ...), custom_call_target="tpu_custom_call" | custom-call | tf_op jit(solution)/shard_map/pallas_call | solution.py:531
Async XLA Ops:
  0.6 1.1 %copy-start = (bf16[256,1536]{1,0:T(8,128)(2,1)S(1)}, bf16[256,1536]{1,0:T(8,128)(2,1)}, u32[]{:S(2)}) copy-start(bf16[256,1536]{1,0:T(8,128)(2,1)} %a_hbm.1) | copy-start | bytes 2359300
  1.8 1.1 %copy-start.1 = (bf16[256,1536]{1,0:T(8,128)(2,1)S(1)}, bf16[256,1536]{1,0:T(8,128)(2,1)}, u32[]{:S(2)}) copy-start(bf16[256,1536]{1,0:T(8,128)(2,1)} %g_hbm.1) | copy-start | bytes 2359300
  2.9 1.1 %copy-start.2 = (bf16[256,1536]{1,0:T(8,128)(2,1)S(1)}, bf16[256,1536]{1,0:T(8,128)(2,1)}, u32[]{:S(2)}) copy-start(bf16[256,1536]{1,0:T(8,128)(2,1)} %cot_hbm.1) | copy-start | bytes 2359300
  4.0 0.9 %copy-start.3 = (bf16[31,1536]{1,0:T(8,128)(2,1)S(1)}, bf16[31,1536]{1,0:T(8,128)(2,1)}, u32[]{:S(2)}) copy-start(bf16[31,1536]{1,0:T(8,128)(2,1)} %taps_hbm.1) | copy-start | bytes 285700
  4.9 0.7 %copy-start.4 = (f32[1536]{0:T(1024)S(1)}, f32[1536]{0:T(1024)}, u32[]{:S(2)}) copy-start(f32[1536]{0:T(1024)} %gain_hbm.1) | copy-start | bytes 18436
  5.6 0.7 %copy-start.5 = (f32[1536]{0:T(1024)S(1)}, f32[1536]{0:T(1024)}, u32[]{:S(2)}) copy-start(f32[1536]{0:T(1024)} %shift_hbm.1) | copy-start | bytes 18436

commit v3 on v2

--- a/solution.py
+++ b/solution.py
@@ -32,11 +32,9 @@
     taps_hbm,
     gain_hbm,
     shift_hbm,
-    ag_out,
-    gg_out,
-    tg_ref,
-    gng_ref,
-    shg_ref,
+    ag_hbm,
+    gg_hbm,
+    full_hbm,
     a_in,
     g_in,
     cot_in,
@@ -74,6 +72,8 @@
     line_rcv,
     full_snd,
     full_rcv,
+    ag_out,
+    gg_out,
     gain_ref,
     shift_ref,
     taps_in,
@@ -84,6 +84,8 @@
     halo_recv,
     red_send,
     red_recv,
+    round_sem,
+    out_sem,
 ):
     nz, ny, nx = sizes
     blocks = ext.shape[0]
@@ -132,20 +134,39 @@
     def greet(device):
         pl.semaphore_signal(barrier, inc=1, device_id=device, device_id_type=MESH)
 
-    greet(other)
-    greet(after)
-    greet(behind)
-
-    for device in line:
+    def along_x(j):
+        return (z, y, lax.rem(x + j + nx, nx), core)
+
+    def along_y(j):
+        return (z, lax.rem(y + j + ny, ny), x, core)
+
+    def along_z(j):
+        return (lax.rem(z + j + nz, nz), y, x, core)
+
+    near = [other, after, behind] + [along(j) for along in (along_x, along_y, along_z) for j in (-1, 1)]
+    for device in near:
         greet(device)
-    for _, device in others:
-        greet(device)
+
+    def tell(index, along, by):
+        for j in (-by, by):
+            pl.semaphore_signal(round_sem.at[index], inc=1, device_id=along(j), device_id_type=MESH)
+
+    def hear(index):
+        pl.semaphore_wait(round_sem.at[index], 2)
 
     loads[0].wait()
     loads[1].wait()
     for c in range(blocks):
         lanes = pl.ds(c * LANES, LANES)
         halo_snd[c] = (a_tail[:, lanes].astype(F32) * sigmoid(g_tail[:, lanes].astype(F32))).astype(BF16)
+
+    pl.semaphore_wait(barrier, len(near))
+    halo = pltpu.make_async_remote_copy(
+        halo_snd, halo_rcv, halo_send.at[0], halo_recv.at[0], device_id=after, device_id_type=MESH
+    )
+    halo.start()
+    tell(0, along_x, 1)
+    tell(1, along_y, 1)
 
     loads[4].wait()
     for c in range(blocks):
@@ -178,11 +199,9 @@
             for r in range(S):
                 ext[c, EDGE + r] = glu[r * S : (r + 1) * S, lanes]
 
-    pl.semaphore_wait(barrier, 3 + (nx - 1) + (plane - 1))
-    halo = pltpu.make_async_remote_copy(
-        halo_snd, halo_rcv, halo_send.at[0], halo_recv.at[0], device_id=after, device_id_type=MESH
-    )
-    halo.start()
+    hear(0)
+    hear(1)
+    tell(2, along_y, 2)
     halo.wait_recv()
     row = lax.broadcasted_iota(jnp.int32, (S, LANES), 0)
 
@@ -199,6 +218,9 @@
             if r >= 2:
                 two = jnp.where(row == 0, halo_f[c, r : r + 1], pltpu.roll(one, 1, 0))
                 ext[c, r - 2] = two.astype(BF16)
+
+    hear(2)
+    tell(3, along_z, 1)
 
     rowsum[...] = jnp.zeros_like(rowsum)
 
@@ -234,6 +256,8 @@
         stat_snd, stat_rcv, tp_send.at[0], tp_recv.at[0], device_id=other, device_id_type=MESH
     )
     stat.start()
+    hear(3)
+    tell(4, along_z, 2)
     stat.wait()
     for r in range(S):
         own_m, far_m = mean_l[r], jnp.broadcast_to(stat_rcv[r][:, 0:1], (S, LANES))
@@ -279,6 +303,8 @@
         sums_snd, sums_rcv, tp_send.at[1], tp_recv.at[1], device_id=other, device_id_type=MESH
     )
     sums.start()
+    hear(4)
+    tell(5, along_z, 1)
     sums.wait()
     for r in range(S):
         both = (sums_snd[r] + sums_rcv[r]) / (2 * chans)
@@ -323,6 +349,7 @@
             part[5 * c + g] = rows.astype(BF16)
         part[5 * c + 4] = jnp.broadcast_to(jnp.sum(col[c, 1], axis=0, keepdims=True), (8, LANES)).astype(BF16)
 
+    hear(5)
     per = part.shape[0] // plane
 
     def shard(index):
@@ -385,6 +412,13 @@
         ag_out[:, wide] = moved(jnp.concatenate(da, axis=1)).astype(BF16)
         gg_out[:, wide] = moved(jnp.concatenate(dg, axis=1)).astype(BF16)
 
+    stores = [
+        pltpu.make_async_copy(ag_out, ag_hbm, out_sem.at[0]),
+        pltpu.make_async_copy(gg_out, gg_hbm, out_sem.at[1]),
+    ]
+    for store in stores:
+        store.start()
+
     def wait_all(ref, count, size, sem):
         some = ref.at[pl.ds(0, count * size)]
         pltpu.make_async_copy(some, some, sem).wait()
@@ -424,6 +458,50 @@
         ).start()
 
     wait_all(full_rcv, plane - 1, per, red_recv.at[2])
+    whole = pltpu.make_async_copy(full_rcv, full_hbm, out_sem.at[2])
+    whole.start()
+    for store in stores:
+        store.wait()
+    halo.wait_send()
+    back.wait_send()
+    wait_all(part, plane - 1, per, red_send.at[0])
+    wait_all(line_rcv, nx - 1, per, red_send.at[1])
+    wait_all(full_rcv, plane - 1, per, red_send.at[2])
+    whole.wait()
+
+
+def put_out(
+    pieces,
+    ag_in,
+    gg_in,
+    full_in,
+    ag_hbm,
+    gg_hbm,
+    tg_hbm,
+    gng_hbm,
+    shg_hbm,
+    ag,
+    gg,
+    full_rcv,
+    tg_ref,
+    gng_ref,
+    shg_ref,
+    in_sem,
+    out_sem,
+):
+    rows = ag.shape[0] // pieces
+    blocks = ag.shape[1] // LANES
+    first = pltpu.make_async_copy(full_in, full_rcv, in_sem.at[2 * pieces])
+    first.start()
+    loads, stores = [], []
+    for i in range(pieces):
+        part = pl.ds(i * rows, rows)
+        for n, (src, held, dst) in enumerate(((ag_in, ag, ag_hbm), (gg_in, gg, gg_hbm))):
+            loads.append(pltpu.make_async_copy(src.at[part], held.at[part], in_sem.at[2 * i + n]))
+            stores.append(pltpu.make_async_copy(held.at[part], dst.at[part], out_sem.at[2 * i + n]))
+    for load in loads:
+        load.start()
+    first.wait()
     for c in range(blocks):
         lanes = slice(c * LANES, (c + 1) * LANES)
         for g in range(4):
@@ -434,22 +512,14 @@
                 tg_ref[24:TAPS, lanes] = rows[:7]
                 gng_ref[lanes] = rows[7:8].reshape(LANES)
         shg_ref[lanes] = full_rcv[5 * c + 4].astype(F32)[0:1].reshape(LANES)
-
-    halo.wait_send()
-    back.wait_send()
-    wait_all(part, plane - 1, per, red_send.at[0])
-    wait_all(line_rcv, nx - 1, per, red_send.at[1])
-    wait_all(full_rcv, plane - 1, per, red_send.at[2])
-
-
-def put_out(*refs):
-    count = len(refs) // 2
-    sem = refs[-1]
-    copies = [pltpu.make_async_copy(refs[i], refs[count + i], sem.at[i]) for i in range(count)]
-    for copy in copies:
-        copy.start()
-    for copy in copies:
-        copy.wait()
+    for n, (held, dst) in enumerate(((tg_ref, tg_hbm), (gng_ref, gng_hbm), (shg_ref, shg_hbm))):
+        stores.append(pltpu.make_async_copy(held, dst, out_sem.at[2 * pieces + n]))
+        stores[-1].start()
+    for load, store in zip(loads, stores):
+        load.wait()
+        store.start()
+    for store in stores:
+        store.wait()
 
 
 def body(sizes, proj_a, proj_gate, taps, norm_gain, norm_shift, cotangent):
@@ -460,7 +530,6 @@
     per = -(-5 * blocks // plane)
     shards = per * plane
     hbm = pl.BlockSpec(memory_space=pltpu.HBM)
-    vmem = pl.BlockSpec(memory_space=pltpu.VMEM)
     tile = (S, S, LANES)
     edge = (blocks, 32, LANES)
     shapes = (
@@ -472,9 +541,9 @@
     )
     outs = pl.pallas_call(
         functools.partial(kernel, sizes),
-        out_shape=shapes,
+        out_shape=(shapes[0], shapes[1], jax.ShapeDtypeStruct((shards, 8, LANES), BF16)),
         in_specs=[hbm] * 6,
-        out_specs=(vmem,) * 5,
+        out_specs=(hbm,) * 3,
         scratch_shapes=[
             pltpu.VMEM((rows, chans), BF16),
             pltpu.VMEM((rows, chans), BF16),
@@ -513,6 +582,8 @@
             pltpu.VMEM((nx * per, 8, LANES), F32),
             pltpu.VMEM((per, 8, LANES), BF16),
             pltpu.VMEM((shards, 8, LANES), BF16),
+            pltpu.VMEM((rows, chans), BF16),
+            pltpu.VMEM((rows, chans), BF16),
             pltpu.VMEM((chans,), F32),
             pltpu.VMEM((chans,), F32),
             pltpu.VMEM((TAPS, chans), BF16),
@@ -523,18 +594,27 @@
             pltpu.SemaphoreType.DMA((2,)),
             pltpu.SemaphoreType.DMA((3,)),
             pltpu.SemaphoreType.DMA((3,)),
+            pltpu.SemaphoreType.REGULAR((6,)),
+            pltpu.SemaphoreType.DMA((3,)),
         ],
         compiler_params=pltpu.CompilerParams(
-            collective_id=0, has_side_effects=True, vmem_limit_bytes=50_000_000
+            collective_id=0, has_side_effects=True, vmem_limit_bytes=64_000_000
         ),
     )(proj_a, proj_gate, cotangent, taps, norm_gain, norm_shift)
+    pieces = 4
     return pl.pallas_call(
-        put_out,
+        functools.partial(put_out, pieces),
         out_shape=shapes,
-        in_specs=[vmem] * 5,
+        in_specs=[hbm] * 3,
         out_specs=(hbm,) * 5,
-        scratch_shapes=[pltpu.SemaphoreType.DMA((5,))],
-        compiler_params=pltpu.CompilerParams(vmem_limit_bytes=16 * 1024 * 1024),
+        scratch_shapes=[
+            *(pltpu.VMEM(shape.shape, shape.dtype) for shape in shapes[:2]),
+            pltpu.VMEM((shards, 8, LANES), BF16),
+            *(pltpu.VMEM(shape.shape, shape.dtype) for shape in shapes[2:]),
+            pltpu.SemaphoreType.DMA((2 * pieces + 1,)),
+            pltpu.SemaphoreType.DMA((2 * pieces + 3,)),
+        ],
+        compiler_params=pltpu.CompilerParams(vmem_limit_bytes=64_000_000),
     )(*outs)
 
 

time: 58.3 us -> 49.4 us (0.85)
  local copies, waits for them, and re-layouts: 5.68 us -> 0 us
  Pallas kernels: 51.6 us -> 48.6 us
    unnamed x12 -> x0, local copies, waits for them, and re-layouts: 5.68 us -> none
    pallas_call x2, Pallas kernels: 51.6 us -> 48.6 us  [the longest x1 46.2 us: body(): pl.pallas_call(functools.partial(kernel, sizes), out_shape=(shapes[0], sh...]
where the time goes in v3:
time: 49.4 us; the launch traced here: 49.2 us
  Pallas kernels  48.6 us (98%)
  between operations  0.64 us (1%)
    pallas_call x1, Pallas kernels, body(): pl.pallas_call(functools.partial(kernel, sizes), out_shape=(shapes[0], sh...  46.2 us
    pallas_call x1, Pallas kernels, body(): pl.pallas_call(functools.partial(put_out, pieces), out_shape=shapes, in_s...  2.37 us

profile of v3, /device:TPU:8, one launch (start us, length us, event | category | flops | bytes accessed | tf_op | source)
XLA Modules:
  0.0 49.2 jit_solution(10592618749772568389)
XLA Ops:
  0.6 46.2 %shard_map.101 = (bf16[256,1536]{1,0:T(8,128)(2,1)}, bf16[256,1536]{1,0:T(8,128)(2,1)}, bf16[64,8,128]{2,1,0:T(8,128)(2,1)}) custom-call(bf16[256,1536]{1,0:T(8,128)(2,1)} %a_hbm.1, bf16[256,1536]{1,0:T(8,128)(2,1)} %g_hbm.1, bf16[256,1536]{1,0:T(8,128)(2,1)} %cot_hbm.1, bf16[31,1536]{1,0:T(8,128)(2,1)} %taps_hbm.1, f32[1536]{0:T(1024)} %gain_hbm.1, ...), custom_call_target="tpu_custom_call" | custom-call | tf_op jit(solution)/shard_map/pallas_call | solution.py:542
  46.8 2.4 %shard_map.102 = (bf16[256,1536]{1,0:T(8,128)(2,1)}, bf16[256,1536]{1,0:T(8,128)(2,1)}, f32[31,1536]{1,0:T(8,128)}, f32[1536]{0:T(1024)}, f32[1536]{0:T(1024)}) custom-call(bf16[256,1536]{1,0:T(8,128)(2,1)} %get-tuple-element.8.ag_in, bf16[256,1536]{1,0:T(8,128)(2,1)} %get-tuple-element.9.gg_in, bf16[64,8,128]{2,1,0:T(8,128)(2,1)} %get-tuple-element.10.full_in), custom_call_target="tpu_custom_call" | custom-call | tf_op jit(solution)/shard_map/pallas_call | solution.py:605

commit v4 on v3

v4 whole, which is shorter than its diff:
```python
import functools

import jax
import jax.numpy as jnp
from jax import lax
from jax.experimental import pallas as pl
from jax.experimental.pallas import tpu as pltpu
from jax.sharding import Mesh
from jax.sharding import PartitionSpec as P

SP = ("sp_0", "sp_1", "sp_2")
EPS = 1e-05
F32 = jnp.float32
BF16 = jnp.bfloat16
MESH = pl.DeviceIdType.MESH
S = 16
RUN = 14
HEAD = 32
LANES = 128
ROWS = 256
EDGE = 30
TAPS = 31


def sigmoid(x):
    return 0.5 * jnp.tanh(0.5 * x) + 0.5


def kernel(
    sizes,
    a_hbm,
    g_hbm,
    cot_hbm,
    taps_hbm,
    gain_hbm,
    shift_hbm,
    ag_hbm,
    gg_hbm,
    full_hbm,
    a_in,
    g_in,
    cot_in,
    a_tail,
    g_tail,
    sg,
    glu_n,
    work,
    dconv_n,
    ext,
    hext,
    dce,
    hdce,
    tapb,
    convs,
    dnorm,
    rowsum,
    rowdot,
    mean_l,
    rstd_s,
    m1_s,
    m2_s,
    stat_snd,
    stat_rcv,
    sums_snd,
    sums_rcv,
    halo_snd,
    halo_rcv,
    back_snd,
    back_rcv,
    col,
    red,
    part,
    part_rcv,
    line_snd,
    line_rcv,
    full_snd,
    ag_out,
    gg_out,
    gain_ref,
    shift_ref,
    taps_in,
    in_sem,
    tp_send,
    tp_recv,
    halo_send,
    halo_recv,
    red_send,
    red_recv,
    round_sem,
    out_sem,
):
    nz, ny, nx = sizes
    blocks = ext.shape[0]
    pieces = halo_send.shape[0] - 1
    group = blocks // pieces
    per = full_snd.shape[0]
    shards = part.shape[0]
    owners = shards // per
    chans = blocks * LANES
    plane = nz * ny
    z, y, x, core = (lax.axis_index(name) for name in (*SP, "tp"))
    sp = (z * ny + y) * nx + x
    total = plane * nx

    def place(index):
        return (index // (ny * nx), index // nx % ny, index % nx, core)

    after = place(lax.rem(sp + 1, total))
    behind = place(lax.rem(sp + total - 1, total))
    other = (z, y, x, 1 - core)
    mine = z * ny + y

    zs = [lax.rem(z + j, nz) for j in range(nz)]
    ys = [lax.rem(y + j, ny) for j in range(ny)]
    line = [(z, y, lax.rem(x + j, nx), core) for j in range(1, nx)]

    def far(n, j):
        return min(j, n - j)

    steps = sorted(
        ((j, i) for j in range(nz) for i in range(ny) if (j, i) != (0, 0)), key=lambda v: -far(nz, v[0]) - far(ny, v[1])
    )
    others = [(zs[j], ys[i], x, core) for j, i in steps]

    tail = pl.ds(ROWS - 32, 32)
    loads = [
        pltpu.make_async_copy(a_hbm.at[tail], a_tail, in_sem.at[0]),
        pltpu.make_async_copy(g_hbm.at[tail], g_tail, in_sem.at[1]),
        pltpu.make_async_copy(taps_hbm, taps_in, in_sem.at[2]),
        pltpu.make_async_copy(a_hbm, a_in, in_sem.at[3]),
        pltpu.make_async_copy(g_hbm, g_in, in_sem.at[4]),
        pltpu.make_async_copy(cot_hbm, cot_in, in_sem.at[5]),
        pltpu.make_async_copy(gain_hbm, gain_ref, in_sem.at[6]),
        pltpu.make_async_copy(shift_hbm, shift_ref, in_sem.at[7]),
    ]
    for load in loads:
        load.start()

    barrier = pltpu.get_barrier_semaphore()

    def greet(device):
        pl.semaphore_signal(barrier, inc=1, device_id=device, device_id_type=MESH)

    def along_x(j):
        return (z, y, lax.rem(x + j + nx, nx), core)

    sides = [along_x(-1), along_x(1)]
    lower = [z >= by for by in (1, 2)]
    upper = [z + by < nz for by in (1, 2)]
    first_sp, last_sp = sp == 0, sp == total - 1

    def around(by, signal):
        def row(j):
            return [(lax.rem(z + j * by + nz, nz), lax.rem(y + i * by + ny, ny), x, core) for i in (-1, 0, 1)]

        for device in row(0)[::2]:
            signal(device)

        @pl.when(lower[by - 1])
        def _():
            for device in row(-1):
                signal(device)

        @pl.when(upper[by - 1])
        def _():
            for device in row(1):
                signal(device)

    def count(by):
        return 2 + jnp.where(lower[by - 1], 3, 0) + jnp.where(upper[by - 1], 3, 0)

    def to_round(index):
        def signal(device):
            pl.semaphore_signal(round_sem.at[index], inc=1, device_id=device, device_id_type=MESH)

        return signal

    greet(other)
    for device in sides:
        greet(device)
    around(1, greet)

    @pl.when(jnp.logical_not(last_sp))
    def _():
        greet(after)

    @pl.when(jnp.logical_not(first_sp))
    def _():
        greet(behind)

    loads[0].wait()
    loads[1].wait()
    for c in range(blocks):
        lanes = pl.ds(c * LANES, LANES)
        halo_snd[c] = (a_tail[:, lanes].astype(F32) * sigmoid(g_tail[:, lanes].astype(F32))).astype(BF16)

    def halo(i):
        piece = pl.ds(i * group, group)
        return pltpu.make_async_remote_copy(
            halo_snd.at[piece],
            halo_rcv.at[piece],
            halo_send.at[i],
            halo_recv.at[i],
            device_id=after,
            device_id_type=MESH,
        )

    def enter():
        pl.semaphore_wait(barrier, 3 + count(1) + jnp.where(first_sp, 0, 1) + jnp.where(last_sp, 0, 1))

        @pl.when(jnp.logical_not(last_sp))
        def _():
            for i in range(pieces):
                halo(i).start()

        for device in sides:
            to_round(0)(device)
        around(1, to_round(0))

    first_x = x == 0

    @pl.when(jnp.logical_not(first_x))
    def _():
        enter()

    loads[2].wait()
    for c in range(blocks):
        rows = taps_in[:, c * LANES : (c + 1) * LANES].astype(F32)
        for k in range(TAPS):
            tapb[c, k] = jnp.broadcast_to(rows[k : k + 1], (S, LANES)).astype(BF16)

    loads[3].wait()
    loads[4].wait()

    def lanes_of(c):
        return pl.ds(pl.multiple_of(c * LANES, LANES), LANES)

    @pl.loop(0, blocks)
    def _(c):
        sv = sigmoid(g_in[:, lanes_of(c)].astype(F32))
        sg[c] = sv
        glu_n[c, HEAD:] = (a_in[:, lanes_of(c)].astype(F32) * sv).astype(BF16).astype(F32)

    @pl.loop(0, blocks)
    def _(c):
        for e in range(-EDGE, RUN):
            ext[c, e + EDGE] = glu_n[c, pl.ds(2 * HEAD + e, S, stride=RUN), :].astype(BF16)

    rowsum[...] = jnp.zeros_like(rowsum)

    def convolve(c, source, first, count, start):
        for q in range(0, count, 4):
            some = range(min(4, count - q))
            acc = [None] * len(some)
            for k in range(TAPS):
                tap = tapb[c, k].astype(F32)
                for m in some:
                    v = source[c, start(q + m, k)].astype(F32) * tap
                    acc[m] = v if acc[m] is None else acc[m] + v
            for m in some:
                yield first + q + m, acc[m]

    @pl.loop(0, blocks)
    def _(c):
        for r, v in convolve(c, ext, 0, RUN, lambda r, k: r + k):
            convs[c, r] = v
            rowsum[r] += v

    lane = lax.broadcasted_iota(jnp.int32, (S, LANES), 1)

    def exchange(snd, rcv, first, count, index):
        some = pl.ds(first, count)
        return pltpu.make_async_remote_copy(
            snd.at[some], rcv.at[some], tp_send.at[index], tp_recv.at[index], device_id=other, device_id_type=MESH
        )

    def figures(first, count, index):
        for r in range(first, first + count):
            mean_l[r] = jnp.broadcast_to(jnp.sum(rowsum[r], axis=1, keepdims=True) / chans, (S, LANES))

        @pl.loop(first, first + count)
        def _(r):
            m = mean_l[r]
            acc = jnp.zeros((S, LANES), F32)
            for c in range(blocks):
                cent = convs[c, r] - m
                acc = acc + cent * cent
            rowdot[r] = acc

        for r in range(first, first + count):
            stat_snd[r] = jnp.where(lane == 0, mean_l[r], jnp.sum(rowdot[r], axis=1, keepdims=True))
        return exchange(stat_snd, stat_rcv, first, count, index)

    def joined(first, count):
        for r in range(first, first + count):
            own_m, far_m = mean_l[r], jnp.broadcast_to(stat_rcv[r][:, 0:1], (S, LANES))
            own_q, far_q = stat_snd[r][:, 1:2], stat_rcv[r][:, 1:2]
            diff = own_m - far_m
            spread = (own_q + far_q + diff * diff * (chans / 2)) / (2 * chans)
            mean_l[r] = 0.5 * (own_m + far_m)
            rstd_s[r] = lax.rsqrt(spread + EPS)

    def swish(r, at):
        m, rs = mean_l[r], rstd_s[r]
        acc1 = jnp.zeros((S, LANES), F32)
        acc2 = jnp.zeros((S, LANES), F32)
        for c in range(blocks):
            lanes = slice(c * LANES, (c + 1) * LANES)
            normed = (convs[c, r] - m) * rs
            gain = gain_ref[lanes].reshape(1, LANES)
            half = normed * (0.5 * gain) + 0.5 * shift_ref[lanes].reshape(1, LANES)
            th = jnp.tanh(half)
            dpre = work[c, at, :] * (1.0 + th) * (1.0 + (half - half * th))
            dn = dpre * gain
            convs[c, r] = normed
            dnorm[c, r] = dn
            acc1 = acc1 + dn
            acc2 = acc2 + dn * normed
            prod = dpre * normed
            col[c, 0] += prod[:8] + prod[8:]
            col[c, 1] += dpre[:8] + dpre[8:]
        rowsum[r] = acc1
        rowdot[r] = acc2

    def sum_figures(first, count, index):
        for r in range(first, first + count):
            sums_snd[r] = jnp.where(
                lane == 0,
                jnp.sum(rowsum[r], axis=1, keepdims=True),
                jnp.sum(rowdot[r], axis=1, keepdims=True),
            )
        copy = exchange(sums_snd, sums_rcv, first, count, index)
        copy.start()
        return copy

    def sums_joined(first, count):
        for r in range(first, first + count):
            both = (sums_snd[r] + sums_rcv[r]) / (2 * chans)
            rs = rstd_s[r]
            m1_s[r] = rs * both[:, 0:1]
            m2_s[r] = rs * both[:, 1:2]

    def dconv(c, r):
        return rstd_s[r] * dnorm[c, r] - m1_s[r] - convs[c, r] * m2_s[r]

    def body_at(r):
        return pl.ds(HEAD + r, S, stride=RUN)

    def head_at(r):
        return pl.ds(r, S, stride=HEAD // S)

    stat = figures(0, RUN, 0)

    @pl.when(first_x)
    def _():
        enter()

    stat.start()
    for i in (5, 6, 7):
        loads[i].wait()

    @pl.loop(0, blocks)
    def _(c):
        work[c] = 0.5 * cot_in[:, lanes_of(c)].astype(F32)

    stat.wait()
    pl.semaphore_wait(round_sem.at[0], 2 + count(1))
    around(2, to_round(1))
    joined(0, RUN)
    col[...] = jnp.zeros_like(col)

    @pl.loop(0, RUN)
    def _(r):
        swish(r, body_at(r))

    sums = sum_figures(0, RUN, 1)

    @pl.when(first_sp)
    def _():
        glu_n[:, :HEAD] = jnp.zeros((blocks, HEAD, LANES), F32)

    @pl.when(jnp.logical_not(first_sp))
    def _():
        for i in range(pieces):
            halo(i).wait_recv()

        @pl.loop(0, blocks)
        def _(c):
            glu_n[c, :HEAD] = halo_rcv[c].astype(F32)

    @pl.loop(0, blocks)
    def _(c):
        for e in range(-EDGE, 2):
            hext[c, e + EDGE] = glu_n[c, pl.ds(HEAD + e, S, stride=2), :].astype(BF16)

    @pl.loop(0, blocks)
    def _(c):
        for r, v in convolve(c, hext, RUN, 2, lambda r, k: r + k):
            convs[c, r] = v
            rowsum[r] = jnp.where(c == 0, v, rowsum[r] + v)

    head_stat = figures(RUN, 2, 2)
    head_stat.start()
    sums.wait()
    pl.semaphore_wait(round_sem.at[1], count(2))
    to_round(2)((lax.rem(z + nz // 2, nz), y, x, core))
    sums_joined(0, RUN)

    @pl.loop(0, blocks)
    def _(c):
        for r in range(RUN):
            d = dconv(c, r)
            dce[c, r] = d.astype(BF16)
            dconv_n[c, body_at(r), :] = d

    head_stat.wait()
    joined(RUN, 2)
    for r in range(2):
        swish(RUN + r, head_at(r))
    head_sums = sum_figures(RUN, 2, 3)
    sub = lax.broadcasted_iota(jnp.int32, (8, LANES), 0)
    for q in range(shards - 4 * blocks):
        rows = jnp.zeros((8, LANES), F32)
        for c in range(8 * q, min(8 * q + 8, blocks)):
            rows = jnp.where(sub == c % 8, jnp.sum(col[c, 1], axis=0, keepdims=True), rows)
        part[4 * blocks + q] = rows.astype(BF16)
    def correlate(c, rows, store):
        for q in range(8):
            ks = [k for k in range(q * 4, q * 4 + 4) if k < TAPS]
            acc = [None] * len(ks)
            for r in rows:
                d = (dce[c, r] if r < RUN else hdce[c, r - RUN]).astype(F32)
                for m, k in enumerate(ks):
                    g = ext[c, k + r] if r < RUN else hext[c, k + r - RUN]
                    v = g.astype(F32) * d
                    acc[m] = v if acc[m] is None else acc[m] + v
            for m, k in enumerate(ks):
                store(pl.ds(9 * k, 8), acc[m][:8] + acc[m][8:])

    @pl.loop(0, blocks)
    def _(c):
        def store(at, v):
            red[c, at, :] = v

        correlate(c, range(RUN - 2), store)

    head_sums.wait()
    sums_joined(RUN, 2)

    @pl.loop(0, blocks)
    def _(c):
        for r in range(2):
            d = dconv(c, RUN + r)
            hdce[c, r] = d.astype(BF16)
            dconv_n[c, head_at(r), :] = d
        back_snd[c] = dconv_n[c, :HEAD].astype(BF16)

    back = pltpu.make_async_remote_copy(
        back_snd, back_rcv, halo_send.at[pieces], halo_recv.at[pieces], device_id=behind, device_id_type=MESH
    )

    @pl.when(jnp.logical_not(first_sp))
    def _():
        back.start()


    @pl.loop(0, blocks)
    def _(c):
        def store(at, v):
            red[c, at, :] += v

        correlate(c, range(RUN - 2, S), store)
        red[c, pl.ds(9 * TAPS, 8), :] = col[c, 0]
        for g in range(4):
            rows = red[c, pl.ds(72 * g, 8, stride=9), :]
            for s in range(1, 8):
                rows = rows + red[c, pl.ds(72 * g + s, 8, stride=9), :]
            part[4 * c + g] = rows.astype(BF16)

    pl.semaphore_wait(round_sem.at[2], 1)

    def shard(index):
        return pl.ds(index * per, per)

    for device in others:
        owner = device[0] * ny + device[1]

        @pl.when(owner < owners)
        def _():
            pltpu.make_async_remote_copy(
                part.at[shard(owner)],
                part_rcv.at[shard(mine)],
                red_send.at[0],
                red_recv.at[0],
                device_id=device,
                device_id_type=MESH,
            ).start()

    def wait_all(ref, count, sem):
        some = ref.at[pl.ds(0, count * per)]
        pltpu.make_async_copy(some, some, sem).wait()

    @pl.when(mine < owners)
    def _():
        part_rcv[shard(mine)] = part[shard(mine)]
        wait_all(part_rcv, plane - 1, red_recv.at[0])
        sums8 = part_rcv[pl.ds(0, per)].astype(F32)
        for j in range(1, plane):
            sums8 = sums8 + part_rcv[pl.ds(j * per, per)].astype(F32)
        line_snd[...] = sums8
        line_rcv[shard(x)] = sums8
        for device in line:
            pltpu.make_async_remote_copy(
                line_snd,
                line_rcv.at[shard(x)],
                red_send.at[1],
                red_recv.at[1],
                device_id=device,
                device_id_type=MESH,
            ).start()
        wait_all(line_rcv, nx - 1, red_recv.at[1])
        sums8 = line_rcv[pl.ds(0, per)]
        for j in range(1, nx):
            sums8 = sums8 + line_rcv[pl.ds(j * per, per)]
        full_snd[...] = sums8.astype(BF16)
        pltpu.make_async_copy(full_snd, full_hbm.at[shard(mine)], out_sem.at[2]).start()
        for device in others:
            pltpu.make_async_remote_copy(
                full_snd,
                full_hbm.at[shard(mine)],
                red_send.at[2],
                red_recv.at[2],
                device_id=device,
                device_id_type=MESH,
            ).start()


    @pl.when(last_sp)
    def _():
        dconv_n[:, ROWS:] = jnp.zeros((blocks, HEAD, LANES), F32)

    @pl.when(jnp.logical_not(last_sp))
    def _():
        back.wait_recv()

        @pl.loop(0, blocks)
        def _(c):
            dconv_n[c, ROWS:] = back_rcv[c].astype(F32)

    @pl.loop(0, blocks)
    def _(c):
        for e in range(RUN, RUN + EDGE):
            dce[c, e] = dconv_n[c, body_at(e), :].astype(BF16)
        for e in range(2, HEAD):
            hdce[c, e] = dconv_n[c, head_at(e), :].astype(BF16)

    @pl.loop(0, blocks)
    def _(c):
        for r, v in convolve(c, dce, 0, RUN, lambda r, k: r + EDGE - k):
            work[c, body_at(r), :] = v
        for r, v in convolve(c, hdce, 0, 2, lambda r, k: r + EDGE - k):
            work[c, head_at(r), :] = v

    @pl.loop(0, blocks)
    def _(c):
        sv = sg[c]
        first = work[c] * sv
        ag_out[:, lanes_of(c)] = first.astype(BF16)
        gg_out[:, lanes_of(c)] = (first * a_in[:, lanes_of(c)].astype(F32) * (1.0 - sv)).astype(BF16)

    stores = [
        pltpu.make_async_copy(ag_out, ag_hbm, out_sem.at[0]),
        pltpu.make_async_copy(gg_out, gg_hbm, out_sem.at[1]),
    ]
    for store in stores:
        store.start()

    @pl.when(mine < owners)
    def _():
        wait_all(full_hbm, owners - 1, red_recv.at[2])
        pltpu.make_async_copy(full_snd, full_hbm.at[shard(mine)], out_sem.at[2]).wait()

    @pl.when(mine >= owners)
    def _():
        wait_all(full_hbm, owners, red_recv.at[2])


    @pl.when(jnp.logical_not(last_sp))
    def _():
        for i in range(pieces):
            halo(i).wait_send()

    @pl.when(jnp.logical_not(first_sp))
    def _():
        back.wait_send()

    @pl.when(mine < owners)
    def _():
        wait_all(part, owners - 1, red_send.at[0])
        wait_all(line_rcv, nx - 1, red_send.at[1])
        wait_all(part_rcv, plane - 1, red_send.at[2])

    @pl.when(mine >= owners)
    def _():
        wait_all(part, owners, red_send.at[0])

    for store in stores:
        store.wait()


def put_out(
    pieces,
    ag_in,
    gg_in,
    full_in,
    ag_hbm,
    gg_hbm,
    tg_hbm,
    gng_hbm,
    shg_hbm,
    ag,
    gg,
    full_rcv,
    tg_ref,
    gng_ref,
    shg_ref,
    in_sem,
    out_sem,
):
    rows = ag.shape[0] // pieces
    blocks = ag.shape[1] // LANES
    first = pltpu.make_async_copy(full_in, full_rcv, in_sem.at[2 * pieces])
    first.start()
    loads, stores = [], []
    for i in range(pieces):
        part = pl.ds(i * rows, rows)
        for n, (src, held, dst) in enumerate(((ag_in, ag, ag_hbm), (gg_in, gg, gg_hbm))):
            loads.append(pltpu.make_async_copy(src.at[part], held.at[part], in_sem.at[2 * i + n]))
            stores.append(pltpu.make_async_copy(held.at[part], dst.at[part], out_sem.at[2 * i + n]))
    for load in loads:
        load.start()
    first.wait()
    for c in range(blocks):
        lanes = slice(c * LANES, (c + 1) * LANES)
        for g in range(4):
            rows = full_rcv[4 * c + g].astype(F32)
            if g < 3:
                tg_ref[8 * g : 8 * g + 8, lanes] = rows
            else:
                tg_ref[24:TAPS, lanes] = rows[:7]
                gng_ref[lanes] = rows[7:8].reshape(LANES)
        row = full_rcv[4 * blocks + c // 8].astype(F32)[c % 8 : c % 8 + 1]
        shg_ref[lanes] = row.reshape(LANES)
    for n, (held, dst) in enumerate(((tg_ref, tg_hbm), (gng_ref, gng_hbm), (shg_ref, shg_hbm))):
        stores.append(pltpu.make_async_copy(held, dst, out_sem.at[2 * pieces + n]))
        stores[-1].start()
    for load, store in zip(loads, stores):
        load.wait()
        store.start()
    for store in stores:
        store.wait()


def body(sizes, proj_a, proj_gate, taps, norm_gain, norm_shift, cotangent):
    rows, chans = proj_a.shape
    blocks = chans // LANES
    nz, ny, nx = sizes
    plane = nz * ny
    shards = 4 * blocks + -(-blocks // 8)
    per = -(-shards // plane)
    assert shards % per == 0
    hbm = pl.BlockSpec(memory_space=pltpu.HBM)
    tile = (S, S, LANES)
    edge = (blocks, 32, LANES)
    shapes = (
        jax.ShapeDtypeStruct((rows, chans), BF16),
        jax.ShapeDtypeStruct((rows, chans), BF16),
        jax.ShapeDtypeStruct((TAPS, chans), F32),
        jax.ShapeDtypeStruct((chans,), F32),
        jax.ShapeDtypeStruct((chans,), F32),
    )
    outs = pl.pallas_call(
        functools.partial(kernel, sizes),
        out_shape=(shapes[0], shapes[1], jax.ShapeDtypeStruct((shards, 8, LANES), BF16)),
        in_specs=[hbm] * 6,
        out_specs=(hbm,) * 3,
        scratch_shapes=[
            pltpu.VMEM((rows, chans), BF16),
            pltpu.VMEM((rows, chans), BF16),
            pltpu.VMEM((rows, chans), BF16),
            pltpu.VMEM((32, chans), BF16),
            pltpu.VMEM((32, chans), BF16),
            pltpu.VMEM((blocks, rows, LANES), F32),
            pltpu.VMEM((blocks, HEAD + rows, LANES), F32),
            pltpu.VMEM((blocks, rows, LANES), F32),
            pltpu.VMEM((blocks, rows + HEAD, LANES), F32),
            pltpu.VMEM((blocks, EDGE + RUN, S, LANES), BF16),
            pltpu.VMEM((blocks, EDGE + 2, S, LANES), BF16),
            pltpu.VMEM((blocks, EDGE + RUN, S, LANES), BF16),
            pltpu.VMEM((blocks, EDGE + 2, S, LANES), BF16),
            pltpu.VMEM((blocks, TAPS, S, LANES), BF16),
            pltpu.VMEM((blocks, *tile), F32),
            pltpu.VMEM((blocks, *tile), F32),
            pltpu.VMEM(tile, F32),
            pltpu.VMEM(tile, F32),
            pltpu.VMEM(tile, F32),
            pltpu.VMEM(tile, F32),
            pltpu.VMEM(tile, F32),
            pltpu.VMEM(tile, F32),
            pltpu.VMEM(tile, F32),
            pltpu.VMEM(tile, F32),
            pltpu.VMEM(tile, F32),
            pltpu.VMEM(tile, F32),
            pltpu.VMEM(edge, BF16),
            pltpu.VMEM(edge, BF16),
            pltpu.VMEM(edge, BF16),
            pltpu.VMEM(edge, BF16),
            pltpu.VMEM((blocks, 2, 8, LANES), F32),
            pltpu.VMEM((blocks, 9 * 32, LANES), F32),
            pltpu.VMEM((shards, 8, LANES), BF16),
            pltpu.VMEM((plane * per, 8, LANES), BF16),
            pltpu.VMEM((per, 8, LANES), F32),
            pltpu.VMEM((nx * per, 8, LANES), F32),
            pltpu.VMEM((per, 8, LANES), BF16),
            pltpu.VMEM((rows, chans), BF16),
            pltpu.VMEM((rows, chans), BF16),
            pltpu.VMEM((chans,), F32),
            pltpu.VMEM((chans,), F32),
            pltpu.VMEM((TAPS, chans), BF16),
            pltpu.SemaphoreType.DMA((8,)),
            pltpu.SemaphoreType.DMA((4,)),
            pltpu.SemaphoreType.DMA((4,)),
            pltpu.SemaphoreType.DMA((2,)),
            pltpu.SemaphoreType.DMA((2,)),
            pltpu.SemaphoreType.DMA((3,)),
            pltpu.SemaphoreType.DMA((3,)),
            pltpu.SemaphoreType.REGULAR((3,)),
            pltpu.SemaphoreType.DMA((3,)),
        ],
        compiler_params=pltpu.CompilerParams(
            collective_id=0, has_side_effects=True, vmem_limit_bytes=64_000_000
        ),
    )(proj_a, proj_gate, cotangent, taps, norm_gain, norm_shift)
    pieces = 4
    return pl.pallas_call(
        functools.partial(put_out, pieces),
        out_shape=shapes,
        in_specs=[hbm] * 3,
        out_specs=(hbm,) * 5,
        scratch_shapes=[
            *(pltpu.VMEM(shape.shape, shape.dtype) for shape in shapes[:2]),
            pltpu.VMEM((shards, 8, LANES), BF16),
            *(pltpu.VMEM(shape.shape, shape.dtype) for shape in shapes[2:]),
            pltpu.SemaphoreType.DMA((2 * pieces + 1,)),
            pltpu.SemaphoreType.DMA((2 * pieces + 3,)),
        ],
        compiler_params=pltpu.CompilerParams(vmem_limit_bytes=64_000_000),
    )(*outs)


def solution(mesh):
    sizes = (8, 8, 4)
    torus = Mesh(mesh.devices.reshape(*sizes, mesh.shape["tp"]), (*SP, "tp"))
    return jax.shard_map(
        functools.partial(body, sizes),
        mesh=torus,
        in_specs=(P(SP, "tp"), P(SP, "tp"), P(None, "tp"), P("tp"), P("tp"), P(SP, "tp")),
        out_specs=(P(SP, "tp"), P(SP, "tp"), P(None, "tp"), P("tp"), P("tp")),
        check_vma=False,
    )
```

time: 49.4 us -> 43.7 us (0.88)
  Pallas kernels: 48.6 us -> 42.9 us
    pallas_call x1, Pallas kernels: 46.2 us -> 40.5 us  [body(): pl.pallas_call(functools.partial(kernel, sizes), out_shape=(shapes[0], sh...]
where the time goes in v4:
time: 43.7 us; the launch traced here: 43.5 us
  Pallas kernels  42.9 us (98%)
  between operations  0.64 us (1%)
    pallas_call x1, Pallas kernels, body(): pl.pallas_call(functools.partial(kernel, sizes), out_shape=(shapes[0], sh...  40.5 us
    pallas_call x1, Pallas kernels, body(): pl.pallas_call(functools.partial(put_out, pieces), out_shape=shapes, in_s...  2.38 us

profile of v4, /device:TPU:8, one launch (start us, length us, event | category | flops | bytes accessed | tf_op | source)
XLA Modules:
  0.0 43.5 jit_solution(16018520240594004507)
XLA Ops:
  0.6 40.5 %shard_map.101 = (bf16[256,1536]{1,0:T(8,128)(2,1)}, bf16[256,1536]{1,0:T(8,128)(2,1)}, bf16[50,8,128]{2,1,0:T(8,128)(2,1)}) custom-call(bf16[256,1536]{1,0:T(8,128)(2,1)} %a_hbm.1, bf16[256,1536]{1,0:T(8,128)(2,1)} %g_hbm.1, bf16[256,1536]{1,0:T(8,128)(2,1)} %cot_hbm.1, bf16[31,1536]{1,0:T(8,128)(2,1)} %taps_hbm.1, f32[1536]{0:T(1024)} %gain_hbm.1, ...), custom_call_target="tpu_custom_call" | custom-call | tf_op jit(solution)/shard_map/pallas_call | solution.py:682
  41.1 2.4 %shard_map.102 = (bf16[256,1536]{1,0:T(8,128)(2,1)}, bf16[256,1536]{1,0:T(8,128)(2,1)}, f32[31,1536]{1,0:T(8,128)}, f32[1536]{0:T(1024)}, f32[1536]{0:T(1024)}) custom-call(bf16[256,1536]{1,0:T(8,128)(2,1)} %get-tuple-element.8.ag_in, bf16[256,1536]{1,0:T(8,128)(2,1)} %get-tuple-element.9.gg_in, bf16[50,8,128]{2,1,0:T(8,128)(2,1)} %get-tuple-element.10.full_in), custom_call_target="tpu_custom_call" | custom-call | tf_op jit(solution)/shard_map/pallas_call | solution.py:745

commit v5 on v4

--- a/solution.py
+++ b/solution.py
@@ -34,9 +34,11 @@
     taps_hbm,
     gain_hbm,
     shift_hbm,
-    ag_hbm,
-    gg_hbm,
-    full_hbm,
+    ag_out,
+    gg_out,
+    tg_ref,
+    gng_ref,
+    shg_ref,
     a_in,
     g_in,
     cot_in,
@@ -74,8 +76,7 @@
     line_snd,
     line_rcv,
     full_snd,
-    ag_out,
-    gg_out,
+    full_rcv,
     gain_ref,
     shift_ref,
     taps_in,
@@ -87,7 +88,6 @@
     red_send,
     red_recv,
     round_sem,
-    out_sem,
 ):
     nz, ny, nx = sizes
     blocks = ext.shape[0]
@@ -133,8 +133,8 @@
         pltpu.make_async_copy(gain_hbm, gain_ref, in_sem.at[6]),
         pltpu.make_async_copy(shift_hbm, shift_ref, in_sem.at[7]),
     ]
-    for load in loads:
-        load.start()
+    for i in (0, 1, 2, 3, 4):
+        loads[i].start()
 
     barrier = pltpu.get_barrier_semaphore()
 
@@ -231,6 +231,8 @@
 
     loads[3].wait()
     loads[4].wait()
+    for i in (5, 6, 7):
+        loads[i].start()
 
     def lanes_of(c):
         return pl.ds(pl.multiple_of(c * LANES, LANES), LANES)
@@ -523,11 +525,11 @@
         for j in range(1, nx):
             sums8 = sums8 + line_rcv[pl.ds(j * per, per)]
         full_snd[...] = sums8.astype(BF16)
-        pltpu.make_async_copy(full_snd, full_hbm.at[shard(mine)], out_sem.at[2]).start()
+        full_rcv[shard(mine)] = sums8.astype(BF16)
         for device in others:
             pltpu.make_async_remote_copy(
                 full_snd,
-                full_hbm.at[shard(mine)],
+                full_rcv.at[shard(mine)],
                 red_send.at[2],
                 red_recv.at[2],
                 device_id=device,
@@ -568,78 +570,14 @@
         ag_out[:, lanes_of(c)] = first.astype(BF16)
         gg_out[:, lanes_of(c)] = (first * a_in[:, lanes_of(c)].astype(F32) * (1.0 - sv)).astype(BF16)
 
-    stores = [
-        pltpu.make_async_copy(ag_out, ag_hbm, out_sem.at[0]),
-        pltpu.make_async_copy(gg_out, gg_hbm, out_sem.at[1]),
-    ]
-    for store in stores:
-        store.start()
-
     @pl.when(mine < owners)
     def _():
-        wait_all(full_hbm, owners - 1, red_recv.at[2])
-        pltpu.make_async_copy(full_snd, full_hbm.at[shard(mine)], out_sem.at[2]).wait()
+        wait_all(full_rcv, owners - 1, red_recv.at[2])
 
     @pl.when(mine >= owners)
     def _():
-        wait_all(full_hbm, owners, red_recv.at[2])
-
-
-    @pl.when(jnp.logical_not(last_sp))
-    def _():
-        for i in range(pieces):
-            halo(i).wait_send()
-
-    @pl.when(jnp.logical_not(first_sp))
-    def _():
-        back.wait_send()
-
-    @pl.when(mine < owners)
-    def _():
-        wait_all(part, owners - 1, red_send.at[0])
-        wait_all(line_rcv, nx - 1, red_send.at[1])
-        wait_all(part_rcv, plane - 1, red_send.at[2])
-
-    @pl.when(mine >= owners)
-    def _():
-        wait_all(part, owners, red_send.at[0])
-
-    for store in stores:
-        store.wait()
-
-
-def put_out(
-    pieces,
-    ag_in,
-    gg_in,
-    full_in,
-    ag_hbm,
-    gg_hbm,
-    tg_hbm,
-    gng_hbm,
-    shg_hbm,
-    ag,
-    gg,
-    full_rcv,
-    tg_ref,
-    gng_ref,
-    shg_ref,
-    in_sem,
-    out_sem,
-):
-    rows = ag.shape[0] // pieces
-    blocks = ag.shape[1] // LANES
-    first = pltpu.make_async_copy(full_in, full_rcv, in_sem.at[2 * pieces])
-    first.start()
-    loads, stores = [], []
-    for i in range(pieces):
-        part = pl.ds(i * rows, rows)
-        for n, (src, held, dst) in enumerate(((ag_in, ag, ag_hbm), (gg_in, gg, gg_hbm))):
-            loads.append(pltpu.make_async_copy(src.at[part], held.at[part], in_sem.at[2 * i + n]))
-            stores.append(pltpu.make_async_copy(held.at[part], dst.at[part], out_sem.at[2 * i + n]))
-    for load in loads:
-        load.start()
-    first.wait()
+        wait_all(full_rcv, owners, red_recv.at[2])
+
     for c in range(blocks):
         lanes = slice(c * LANES, (c + 1) * LANES)
         for g in range(4):
@@ -651,14 +589,36 @@
                 gng_ref[lanes] = rows[7:8].reshape(LANES)
         row = full_rcv[4 * blocks + c // 8].astype(F32)[c % 8 : c % 8 + 1]
         shg_ref[lanes] = row.reshape(LANES)
-    for n, (held, dst) in enumerate(((tg_ref, tg_hbm), (gng_ref, gng_hbm), (shg_ref, shg_hbm))):
-        stores.append(pltpu.make_async_copy(held, dst, out_sem.at[2 * pieces + n]))
-        stores[-1].start()
-    for load, store in zip(loads, stores):
-        load.wait()
-        store.start()
-    for store in stores:
-        store.wait()
+
+
+    @pl.when(jnp.logical_not(last_sp))
+    def _():
+        for i in range(pieces):
+            halo(i).wait_send()
+
+    @pl.when(jnp.logical_not(first_sp))
+    def _():
+        back.wait_send()
+
+    @pl.when(mine < owners)
+    def _():
+        wait_all(part, owners - 1, red_send.at[0])
+        wait_all(line_rcv, nx - 1, red_send.at[1])
+        wait_all(part_rcv, plane - 1, red_send.at[2])
+
+    @pl.when(mine >= owners)
+    def _():
+        wait_all(part, owners, red_send.at[0])
+
+
+def put_out(*refs):
+    *refs, sem = refs
+    count = len(refs) // 2
+    copies = [pltpu.make_async_copy(refs[i], refs[count + i], sem.at[i]) for i in range(count)]
+    for copy in copies:
+        copy.start()
+    for copy in copies:
+        copy.wait()
 
 
 def body(sizes, proj_a, proj_gate, taps, norm_gain, norm_shift, cotangent):
@@ -670,6 +630,7 @@
     per = -(-shards // plane)
     assert shards % per == 0
     hbm = pl.BlockSpec(memory_space=pltpu.HBM)
+    vmem = pl.BlockSpec(memory_space=pltpu.VMEM)
     tile = (S, S, LANES)
     edge = (blocks, 32, LANES)
     shapes = (
@@ -681,9 +642,9 @@
     )
     outs = pl.pallas_call(
         functools.partial(kernel, sizes),
-        out_shape=(shapes[0], shapes[1], jax.ShapeDtypeStruct((shards, 8, LANES), BF16)),
+        out_shape=tuple(pltpu.VMEM(shape.shape, shape.dtype) for shape in shapes),
         in_specs=[hbm] * 6,
-        out_specs=(hbm,) * 3,
+        out_specs=(vmem,) * 5,
         scratch_shapes=[
             pltpu.VMEM((rows, chans), BF16),
             pltpu.VMEM((rows, chans), BF16),
@@ -722,8 +683,7 @@
             pltpu.VMEM((per, 8, LANES), F32),
             pltpu.VMEM((nx * per, 8, LANES), F32),
             pltpu.VMEM((per, 8, LANES), BF16),
-            pltpu.VMEM((rows, chans), BF16),
-            pltpu.VMEM((rows, chans), BF16),
+            pltpu.VMEM((shards, 8, LANES), BF16),
             pltpu.VMEM((chans,), F32),
             pltpu.VMEM((chans,), F32),
             pltpu.VMEM((TAPS, chans), BF16),
@@ -735,26 +695,18 @@
             pltpu.SemaphoreType.DMA((3,)),
             pltpu.SemaphoreType.DMA((3,)),
             pltpu.SemaphoreType.REGULAR((3,)),
-            pltpu.SemaphoreType.DMA((3,)),
         ],
         compiler_params=pltpu.CompilerParams(
             collective_id=0, has_side_effects=True, vmem_limit_bytes=64_000_000
         ),
     )(proj_a, proj_gate, cotangent, taps, norm_gain, norm_shift)
-    pieces = 4
     return pl.pallas_call(
-        functools.partial(put_out, pieces),
+        put_out,
         out_shape=shapes,
-        in_specs=[hbm] * 3,
+        in_specs=[vmem] * 5,
         out_specs=(hbm,) * 5,
-        scratch_shapes=[
-            *(pltpu.VMEM(shape.shape, shape.dtype) for shape in shapes[:2]),
-            pltpu.VMEM((shards, 8, LANES), BF16),
-            *(pltpu.VMEM(shape.shape, shape.dtype) for shape in shapes[2:]),
-            pltpu.SemaphoreType.DMA((2 * pieces + 1,)),
-            pltpu.SemaphoreType.DMA((2 * pieces + 3,)),
-        ],
-        compiler_params=pltpu.CompilerParams(vmem_limit_bytes=64_000_000),
+        scratch_shapes=[pltpu.SemaphoreType.DMA((5,))],
+        compiler_params=pltpu.CompilerParams(vmem_limit_bytes=16_000_000),
     )(*outs)
 
 

time: 43.7 us -> 42.4 us (0.970)
  Pallas kernels: 42.9 us -> 41.6 us
    pallas_call x2, Pallas kernels: 42.9 us -> 41.6 us  [the longest x1 40.4 us: body(): pl.pallas_call(functools.partial(kernel, sizes), out_shape=tuple((pltpu.V...]
where the time goes in v5:
time: 42.4 us; the launch traced here: 42.2 us
  Pallas kernels  41.6 us (98%)
  between operations  0.64 us (2%)
    pallas_call x1, Pallas kernels, body(): pl.pallas_call(functools.partial(kernel, sizes), out_shape=tuple((pltpu.V...  40.4 us
    pallas_call x1, Pallas kernels, body(): pl.pallas_call(put_out, out_shape=shapes, in_specs=[vmem] * 5, out_specs=...  1.25 us

profile of v5, /device:TPU:8, one launch (start us, length us, event | category | flops | bytes accessed | tf_op | source)
XLA Modules:
  0.0 42.2 jit_solution(12841042854405594307)
XLA Ops:
  0.6 40.4 %shard_map.101 = (bf16[256,1536]{1,0:T(8,128)(2,1)S(1)}, bf16[256,1536]{1,0:T(8,128)(2,1)S(1)}, f32[31,1536]{1,0:T(8,128)S(1)}, f32[1536]{0:T(1024)S(1)}, f32[1536]{0:T(1024)S(1)}) custom-call(bf16[256,1536]{1,0:T(8,128)(2,1)} %a_hbm.1, bf16[256,1536]{1,0:T(8,128)(2,1)} %g_hbm.1, bf16[256,1536]{1,0:T(8,128)(2,1)} %cot_hbm.1, bf16[31,1536]{1,0:T(8,128)(2,1)} %taps_hbm.1, ...), custom_call_target="tpu_custom_call" | custom-call | tf_op jit(solution)/shard_map/pallas_call | solution.py:643
  41.0 1.2 %shard_map.102 = (bf16[256,1536]{1,0:T(8,128)(2,1)}, bf16[256,1536]{1,0:T(8,128)(2,1)}, f32[31,1536]{1,0:T(8,128)}, f32[1536]{0:T(1024)}, f32[1536]{0:T(1024)}) custom-call(bf16[256,1536]{1,0:T(8,128)(2,1)S(1)} %get-tuple-element.10.refs_0_, bf16[256,1536]{1,0:T(8,128)(2,1)S(1)} %get-tuple-element.11.refs_1_, f32[31,1536]{1,0:T(8,128)S(1)} %get-tuple-element.12.refs_2_, ...), custom_call_target="tpu_custom_call" | custom-call | tf_op jit(solution)/shard_map/pallas_call | solution.py:703

commit v6 on v5

--- a/solution.py
+++ b/solution.py
@@ -127,13 +127,16 @@
         pltpu.make_async_copy(a_hbm.at[tail], a_tail, in_sem.at[0]),
         pltpu.make_async_copy(g_hbm.at[tail], g_tail, in_sem.at[1]),
         pltpu.make_async_copy(taps_hbm, taps_in, in_sem.at[2]),
-        pltpu.make_async_copy(a_hbm, a_in, in_sem.at[3]),
-        pltpu.make_async_copy(g_hbm, g_in, in_sem.at[4]),
-        pltpu.make_async_copy(cot_hbm, cot_in, in_sem.at[5]),
-        pltpu.make_async_copy(gain_hbm, gain_ref, in_sem.at[6]),
-        pltpu.make_async_copy(shift_hbm, shift_ref, in_sem.at[7]),
+        *(
+            pltpu.make_async_copy(src.at[:, half], dst.at[:, half], in_sem.at[3 + 2 * n + m])
+            for n, half in enumerate((pl.ds(0, chans // 2), pl.ds(chans // 2, chans // 2)))
+            for m, (src, dst) in enumerate(((a_hbm, a_in), (g_hbm, g_in)))
+        ),
+        pltpu.make_async_copy(cot_hbm, cot_in, in_sem.at[7]),
+        pltpu.make_async_copy(gain_hbm, gain_ref, in_sem.at[8]),
+        pltpu.make_async_copy(shift_hbm, shift_ref, in_sem.at[9]),
     ]
-    for i in (0, 1, 2, 3, 4):
+    for i in range(7):
         loads[i].start()
 
     barrier = pltpu.get_barrier_semaphore()
@@ -229,19 +232,21 @@
         for k in range(TAPS):
             tapb[c, k] = jnp.broadcast_to(rows[k : k + 1], (S, LANES)).astype(BF16)
 
-    loads[3].wait()
-    loads[4].wait()
-    for i in (5, 6, 7):
-        loads[i].start()
-
     def lanes_of(c):
         return pl.ds(pl.multiple_of(c * LANES, LANES), LANES)
 
-    @pl.loop(0, blocks)
-    def _(c):
-        sv = sigmoid(g_in[:, lanes_of(c)].astype(F32))
-        sg[c] = sv
-        glu_n[c, HEAD:] = (a_in[:, lanes_of(c)].astype(F32) * sv).astype(BF16).astype(F32)
+    for n in range(2):
+        loads[3 + 2 * n].wait()
+        loads[4 + 2 * n].wait()
+        if n:
+            for i in (7, 8, 9):
+                loads[i].start()
+
+        @pl.loop(n * blocks // 2, (n + 1) * blocks // 2)
+        def _(c):
+            sv = sigmoid(g_in[:, lanes_of(c)].astype(F32))
+            sg[c] = sv
+            glu_n[c, HEAD:] = (a_in[:, lanes_of(c)].astype(F32) * sv).astype(BF16).astype(F32)
 
     @pl.loop(0, blocks)
     def _(c):
@@ -270,15 +275,20 @@
 
     lane = lax.broadcasted_iota(jnp.int32, (S, LANES), 1)
 
-    def exchange(snd, rcv, first, count, index):
-        some = pl.ds(first, count)
+    def exchange(snd, rcv, index):
         return pltpu.make_async_remote_copy(
-            snd.at[some], rcv.at[some], tp_send.at[index], tp_recv.at[index], device_id=other, device_id_type=MESH
+            snd, rcv, tp_send.at[index], tp_recv.at[index], device_id=other, device_id_type=MESH
         )
+
+    def packed(pairs):
+        tile = jnp.zeros((S, LANES), F32)
+        for n, (one, two) in enumerate(pairs):
+            tile = jnp.where(lane == 2 * n, one, jnp.where(lane == 2 * n + 1, two, tile))
+        return tile
 
     def figures(first, count, index):
         for r in range(first, first + count):
-            mean_l[r] = jnp.broadcast_to(jnp.sum(rowsum[r], axis=1, keepdims=True) / chans, (S, LANES))
+            mean_l[r] = jnp.broadcast_to(jnp.sum(rowsum[r], axis=1, keepdims=True) * (1.0 / chans), (S, LANES))
 
         @pl.loop(first, first + count)
         def _(r):
@@ -289,18 +299,20 @@
                 acc = acc + cent * cent
             rowdot[r] = acc
 
-        for r in range(first, first + count):
-            stat_snd[r] = jnp.where(lane == 0, mean_l[r], jnp.sum(rowdot[r], axis=1, keepdims=True))
-        return exchange(stat_snd, stat_rcv, first, count, index)
+        stat_snd[index // 2] = packed(
+            (mean_l[r], jnp.sum(rowdot[r], axis=1, keepdims=True)) for r in range(first, first + count)
+        )
+        return exchange(stat_snd.at[index // 2], stat_rcv.at[index // 2], index)
 
     def joined(first, count):
-        for r in range(first, first + count):
-            own_m, far_m = mean_l[r], jnp.broadcast_to(stat_rcv[r][:, 0:1], (S, LANES))
-            own_q, far_q = stat_snd[r][:, 1:2], stat_rcv[r][:, 1:2]
-            diff = own_m - far_m
-            spread = (own_q + far_q + diff * diff * (chans / 2)) / (2 * chans)
-            mean_l[r] = 0.5 * (own_m + far_m)
-            rstd_s[r] = lax.rsqrt(spread + EPS)
+        own, far = stat_snd[first // RUN], stat_rcv[first // RUN]
+        both = own + far
+        diff = own - far
+        for n in range(count):
+            m, q = slice(2 * n, 2 * n + 1), slice(2 * n + 1, 2 * n + 2)
+            spread = (both[:, q] + diff[:, m] * diff[:, m] * (chans / 2)) * (0.5 / chans)
+            mean_l[first + n] = jnp.broadcast_to(0.5 * both[:, m], (S, LANES))
+            rstd_s[first + n] = jnp.broadcast_to(lax.rsqrt(spread + EPS), (S, LANES))
 
     def swish(r, at):
         m, rs = mean_l[r], rstd_s[r]
@@ -325,22 +337,20 @@
         rowdot[r] = acc2
 
     def sum_figures(first, count, index):
-        for r in range(first, first + count):
-            sums_snd[r] = jnp.where(
-                lane == 0,
-                jnp.sum(rowsum[r], axis=1, keepdims=True),
-                jnp.sum(rowdot[r], axis=1, keepdims=True),
-            )
-        copy = exchange(sums_snd, sums_rcv, first, count, index)
+        sums_snd[index // 2] = packed(
+            (jnp.sum(rowsum[r], axis=1, keepdims=True), jnp.sum(rowdot[r], axis=1, keepdims=True))
+            for r in range(first, first + count)
+        )
+        copy = exchange(sums_snd.at[index // 2], sums_rcv.at[index // 2], index)
         copy.start()
         return copy
 
     def sums_joined(first, count):
-        for r in range(first, first + count):
-            both = (sums_snd[r] + sums_rcv[r]) / (2 * chans)
-            rs = rstd_s[r]
-            m1_s[r] = rs * both[:, 0:1]
-            m2_s[r] = rs * both[:, 1:2]
+        both = (sums_snd[first // RUN] + sums_rcv[first // RUN]) * (0.5 / chans)
+        for n in range(count):
+            rs = rstd_s[first + n]
+            m1_s[first + n] = rs * both[:, 2 * n : 2 * n + 1]
+            m2_s[first + n] = rs * both[:, 2 * n + 1 : 2 * n + 2]
 
     def dconv(c, r):
         return rstd_s[r] * dnorm[c, r] - m1_s[r] - convs[c, r] * m2_s[r]
@@ -358,16 +368,16 @@
         enter()
 
     stat.start()
-    for i in (5, 6, 7):
-        loads[i].wait()
-
-    @pl.loop(0, blocks)
-    def _(c):
-        work[c] = 0.5 * cot_in[:, lanes_of(c)].astype(F32)
-
-    stat.wait()
     pl.semaphore_wait(round_sem.at[0], 2 + count(1))
     around(2, to_round(1))
+    for i in (7, 8, 9):
+        loads[i].wait()
+
+    @pl.loop(0, blocks)
+    def _(c):
+        work[c] = 0.5 * cot_in[:, lanes_of(c)].astype(F32)
+
+    stat.wait()
     joined(0, RUN)
     col[...] = jnp.zeros_like(col)
 
@@ -668,10 +678,10 @@
             pltpu.VMEM(tile, F32),
             pltpu.VMEM(tile, F32),
             pltpu.VMEM(tile, F32),
-            pltpu.VMEM(tile, F32),
-            pltpu.VMEM(tile, F32),
-            pltpu.VMEM(tile, F32),
-            pltpu.VMEM(tile, F32),
+            pltpu.VMEM((2, S, LANES), F32),
+            pltpu.VMEM((2, S, LANES), F32),
+            pltpu.VMEM((2, S, LANES), F32),
+            pltpu.VMEM((2, S, LANES), F32),
             pltpu.VMEM(edge, BF16),
             pltpu.VMEM(edge, BF16),
             pltpu.VMEM(edge, BF16),
@@ -687,7 +697,7 @@
             pltpu.VMEM((chans,), F32),
             pltpu.VMEM((chans,), F32),
             pltpu.VMEM((TAPS, chans), BF16),
-            pltpu.SemaphoreType.DMA((8,)),
+            pltpu.SemaphoreType.DMA((10,)),
             pltpu.SemaphoreType.DMA((4,)),
             pltpu.SemaphoreType.DMA((4,)),
             pltpu.SemaphoreType.DMA((2,)),

time: 42.4 us -> 42.1 us (level)
  the two profiles are of different devices: /device:TPU:8 before, /device:TPU:4 now
where the time goes in v6:
time: 42.1 us; the launch traced here: 41.9 us
  Pallas kernels  41.3 us (98%)
  between operations  0.64 us (2%)
    pallas_call x1, Pallas kernels, body(): pl.pallas_call(functools.partial(kernel, sizes), out_shape=tuple((pltpu.V...  40.1 us
    pallas_call x1, Pallas kernels, body(): pl.pallas_call(put_out, out_shape=shapes, in_specs=[vmem] * 5, out_specs=...  1.25 us

profile of v6, /device:TPU:4, one launch (start us, length us, event | category | flops | bytes accessed | tf_op | source)
XLA Modules:
  0.0 41.9 jit_solution(4515014712944489535)
XLA Ops:
  0.6 40.1 %shard_map.101 = (bf16[256,1536]{1,0:T(8,128)(2,1)S(1)}, bf16[256,1536]{1,0:T(8,128)(2,1)S(1)}, f32[31,1536]{1,0:T(8,128)S(1)}, f32[1536]{0:T(1024)S(1)}, f32[1536]{0:T(1024)S(1)}) custom-call(bf16[256,1536]{1,0:T(8,128)(2,1)} %a_hbm.1, bf16[256,1536]{1,0:T(8,128)(2,1)} %g_hbm.1, bf16[256,1536]{1,0:T(8,128)(2,1)} %cot_hbm.1, bf16[31,1536]{1,0:T(8,128)(2,1)} %taps_hbm.1, ...), custom_call_target="tpu_custom_call" | custom-call | tf_op jit(solution)/shard_map/pallas_call | solution.py:653
  40.7 1.2 %shard_map.102 = (bf16[256,1536]{1,0:T(8,128)(2,1)}, bf16[256,1536]{1,0:T(8,128)(2,1)}, f32[31,1536]{1,0:T(8,128)}, f32[1536]{0:T(1024)}, f32[1536]{0:T(1024)}) custom-call(bf16[256,1536]{1,0:T(8,128)(2,1)S(1)} %get-tuple-element.10.refs_0_, bf16[256,1536]{1,0:T(8,128)(2,1)S(1)} %get-tuple-element.11.refs_1_, f32[31,1536]{1,0:T(8,128)S(1)} %get-tuple-element.12.refs_2_, ...), custom_call_target="tpu_custom_call" | custom-call | tf_op jit(solution)/shard_map/pallas_call | solution.py:713

commit v7 on v6

--- a/solution.py
+++ b/solution.py
@@ -405,11 +405,21 @@
         for e in range(-EDGE, 2):
             hext[c, e + EDGE] = glu_n[c, pl.ds(HEAD + e, S, stride=2), :].astype(BF16)
 
-    @pl.loop(0, blocks)
-    def _(c):
-        for r, v in convolve(c, hext, RUN, 2, lambda r, k: r + k):
-            convs[c, r] = v
-            rowsum[r] = jnp.where(c == 0, v, rowsum[r] + v)
+    @pl.loop(0, blocks // 2)
+    def _(n):
+        acc = [None] * 4
+        for k in range(TAPS):
+            for b in range(2):
+                tap = tapb[2 * n + b, k].astype(F32)
+                for r in range(2):
+                    v = hext[2 * n + b, r + k].astype(F32) * tap
+                    m = 2 * b + r
+                    acc[m] = v if acc[m] is None else acc[m] + v
+        for r in range(2):
+            convs[2 * n, RUN + r] = acc[r]
+            convs[2 * n + 1, RUN + r] = acc[2 + r]
+            v = acc[r] + acc[2 + r]
+            rowsum[RUN + r] = jnp.where(n == 0, v, rowsum[RUN + r] + v)
 
     head_stat = figures(RUN, 2, 2)
     head_stat.start()

time: 42.1 us -> 42 us (level)
  no operation moved by 1% of the time
where the time goes in v7:
time: 42 us; the launch traced here: 41.9 us
  Pallas kernels  41.2 us (98%)
  between operations  0.64 us (2%)
    pallas_call x1, Pallas kernels, body(): pl.pallas_call(functools.partial(kernel, sizes), out_shape=tuple((pltpu.V...  40 us
    pallas_call x1, Pallas kernels, body(): pl.pallas_call(put_out, out_shape=shapes, in_specs=[vmem] * 5, out_specs=...  1.25 us

profile of v7, /device:TPU:4, one launch (start us, length us, event | category | flops | bytes accessed | tf_op | source)
XLA Modules:
  0.0 41.9 jit_solution(4307877323641772039)
XLA Ops:
  0.6 40.0 %shard_map.101 = (bf16[256,1536]{1,0:T(8,128)(2,1)S(1)}, bf16[256,1536]{1,0:T(8,128)(2,1)S(1)}, f32[31,1536]{1,0:T(8,128)S(1)}, f32[1536]{0:T(1024)S(1)}, f32[1536]{0:T(1024)S(1)}) custom-call(bf16[256,1536]{1,0:T(8,128)(2,1)} %a_hbm.1, bf16[256,1536]{1,0:T(8,128)(2,1)} %g_hbm.1, bf16[256,1536]{1,0:T(8,128)(2,1)} %cot_hbm.1, bf16[31,1536]{1,0:T(8,128)(2,1)} %taps_hbm.1, ...), custom_call_target="tpu_custom_call" | custom-call | tf_op jit(solution)/shard_map/pallas_call | solution.py:663
  40.6 1.2 %shard_map.102 = (bf16[256,1536]{1,0:T(8,128)(2,1)}, bf16[256,1536]{1,0:T(8,128)(2,1)}, f32[31,1536]{1,0:T(8,128)}, f32[1536]{0:T(1024)}, f32[1536]{0:T(1024)}) custom-call(bf16[256,1536]{1,0:T(8,128)(2,1)S(1)} %get-tuple-element.10.refs_0_, bf16[256,1536]{1,0:T(8,128)(2,1)S(1)} %get-tuple-element.11.refs_1_, f32[31,1536]{1,0:T(8,128)S(1)} %get-tuple-element.12.refs_2_, ...), custom_call_target="tpu_custom_call" | custom-call | tf_op jit(solution)/shard_map/pallas_call | solution.py:723
